TPU v7x, 512 devices: a whole 4x8x8 slice. The times are simulated.
512 devices in a mesh: fs: 64 (over z, y), tp: 8 (over x, core).
Axes of the slice: x: 4, y: 8, z: 8, core: 2. Of those that a mesh axis runs over, the one named last changes fastest.
Arguments:
- inputs: bfloat16 [32768, 2048], P('fs', 'tp'), may hold values from -6 to 6
- value_cotangent: bfloat16 [32768, 2048], P('fs', 'tp'), may hold values from -6 to 6
- first_map: bfloat16 [32768, 2048], P('fs', 'tp'), may hold values from -6 to 6
- second_map: bfloat16 [32768, 2048], P('fs', 'tp'), may hold values from -6 to 6
- lambdas: float32 [16], P('tp'), may hold values from 0.3 to 0.8
- head_gain: float32 [128], replicated, may hold values from 0.1 to 1.9
- output_cotangent: bfloat16 [32768, 2048], P('fs', 'tp'), may hold values from -6 to 6
- value_factor: bfloat16 [2048, 256], replicated, may hold values from -0.125 to 0.125
- output_factor: bfloat16 [2048, 256], replicated, may hold values from -0.125 to 0.125
- value_weight: float32 [2048, 2048], P('fs', 'tp'), may hold values from -0.125 to 0.125
- output_weight: float32 [2048, 2048], P('tp', 'fs'), may hold values from -0.125 to 0.125
- value_moment: float32 [256, 2048], P('fs', 'tp'), may hold values from -6 to 6
- value_second: float32 [256, 2048], P('fs', 'tp'), may hold values from 0.25 to 4
- output_moment: float32 [256, 2048], P('fs', 'tp'), may hold values from -6 to 6
- output_second: float32 [256, 2048], P('fs', 'tp'), may hold values from 0.25 to 4
Outputs:
- value_master: float32 [2048, 2048], P('fs', 'tp')
- output_master: float32 [2048, 2048], P('tp', 'fs')
- value_moment_new: float32 [256, 2048], P('fs', 'tp')
- value_second_new: float32 [256, 2048], P('fs', 'tp')
- output_moment_new: float32 [256, 2048], P('fs', 'tp')
- output_second_new: float32 [256, 2048], P('fs', 'tp')
- value_copy: bfloat16 [2048, 2048], P(None, 'tp')
- output_copy: bfloat16 [2048, 2048], P('tp')
All inputs are finite; a program needn't handle non-finite values.
Results may differ from a plain program's by a relative error of at most 0.0027.
Values may be sent and summed in bfloat16 or wider, within the bound.
No kernel may reach another device: no remote copies, remote signals or barrier semaphores. Data moves between devices by JAX's collectives and lax.ppermute only.
A program may use at most 64 MiB of HBM per device.

v0:
```python
import math

import jax
import jax.numpy as jnp
from jax import lax
from jax.sharding import PartitionSpec as P


def side_by_side(arrays, axis, dim, along):
    ends, at = ([], 0)
    for a in arrays[:-1]:
        at += a.shape[along]
        ends.append(at)
    both = jnp.concatenate(arrays, axis=along)
    return tuple(jnp.split(lax.all_gather(both, axis, axis=dim, tiled=True), ends, axis=along))


def cut_along(x, dim, size):
    before, after = (x.shape[:dim], x.shape[dim + 1 :])
    return jnp.moveaxis(x.reshape(*before, size, -1, *after), dim, 0)


def sum_at_owner(x, axis, dim):
    size = lax.axis_size(axis)
    tiles = lax.all_to_all(cut_along(x, dim, size), axis, 0, 0, tiled=True)
    return jnp.sum(tiles.astype(jnp.float32), axis=0)


def laid_out(tiles, dim):
    tiles = jnp.moveaxis(tiles, 0, dim)
    lengths = tiles.shape
    return tiles.reshape(*lengths[:dim], lengths[dim] * lengths[dim + 1], *lengths[dim + 2 :])


def copy_for_each(x, axis):
    size = lax.axis_size(axis)
    return lax.all_to_all(jnp.broadcast_to(x[None], (size, *x.shape)), axis, 0, 0, tiled=True)


def gathered_copies(x, axis, dim):
    return laid_out(copy_for_each(x, axis), dim)


def gather_turned(arrays, axis, dims):
    turned = [jnp.moveaxis(a, dim, 0) for a, dim in zip(arrays, dims)]
    both = jnp.concatenate([t.reshape(len(t), -1) for t in turned], axis=1)
    filled, at, done = (lax.all_gather(both, axis, axis=0, tiled=True), 0, [])
    for t, dim in zip(turned, dims):
        slab = filled[:, at : at + t[0].size].reshape(-1, *t.shape[1:])
        done.append(jnp.moveaxis(slab, 0, dim))
        at += t[0].size
    return tuple(done)


def contract_rows(left, right, precise):
    if precise:
        return lax.dot_general(
            left,
            right,
            (((0,), (0,)), ((), ())),
            precision=lax.Precision.HIGHEST,
            preferred_element_type=jnp.float32,
        )
    return lax.dot_general(
        left, right, (((0,), (0,)), ((), ())), preferred_element_type=jnp.float32
    )


def local(
    inputs,
    value_cotangent,
    first_map,
    second_map,
    lambdas,
    head_gain,
    output_cotangent,
    value_factor,
    output_factor,
    value_weight,
    output_weight,
    value_moment,
    value_second,
    output_moment,
    output_second,
):
    tok_rows = inputs.shape[0]
    local_heads = lambdas.shape[0]
    head_width = head_gain.shape[0]
    head_cols = local_heads * head_width
    first = first_map.astype(jnp.float32).reshape(tok_rows, local_heads, head_width)
    second = second_map.astype(jnp.float32).reshape(tok_rows, local_heads, head_width)
    difference = first - lambdas[None, :, None] * second
    normed = (
        difference
        * lax.rsqrt(jnp.mean(difference * difference, axis=-1, keepdims=True) + 1e-06)
        * head_gain
    )
    heads_out = normed.reshape(tok_rows, head_cols).astype(jnp.bfloat16)
    full_inputs, full_cotangent = side_by_side((inputs, output_cotangent), "tp", 1, 0)
    token_scale = 1.0 / math.sqrt(tok_rows * lax.axis_size("fs"))
    fs_index = lax.axis_index("fs")
    width_rows = value_weight.shape[0]
    value_rows = lax.dynamic_slice_in_dim(
        value_factor, fs_index * width_rows, width_rows, 0
    ).astype(jnp.float32)
    output_rows = lax.dynamic_slice_in_dim(
        output_factor, fs_index * width_rows, width_rows, 0
    ).astype(jnp.float32)
    grad_value = contract_rows(full_inputs, value_cotangent, False) * token_scale
    grad_output = contract_rows(full_cotangent, heads_out, False) * token_scale
    partial_value = jnp.concatenate(
        [
            contract_rows(value_factor.astype(jnp.float32), grad_value, True),
            contract_rows(output_factor.astype(jnp.float32), grad_output, True),
        ],
        axis=1,
    )
    own_rows = sum_at_owner(partial_value.astype(jnp.bfloat16), "fs", 0)
    moments = jnp.concatenate([value_moment, output_moment], axis=1)
    seconds = jnp.concatenate([value_second, output_second], axis=1)
    moment_new = 0.8 * moments + 0.2 * own_rows
    second_new = 0.95 * seconds + 0.05 * own_rows * own_rows
    direction = moment_new / (jnp.sqrt(second_new) + 1e-08)
    full_direction = gathered_copies(direction, "fs", 0)
    step_value = jnp.dot(
        value_rows,
        full_direction[:, :head_cols],
        precision=lax.Precision.HIGHEST,
        preferred_element_type=jnp.float32,
    )
    step_output = jnp.dot(
        output_rows,
        full_direction[:, head_cols:],
        precision=lax.Precision.HIGHEST,
        preferred_element_type=jnp.float32,
    )
    value_master = value_weight - 0.05 * step_value
    output_master = output_weight - 0.05 * step_output.T
    value_copy, output_copy = gather_turned(
        (value_master.astype(jnp.bfloat16), output_master.astype(jnp.bfloat16)), "fs", (0, 1)
    )
    return (
        value_master,
        output_master,
        moment_new[:, :head_cols],
        second_new[:, :head_cols],
        moment_new[:, head_cols:],
        second_new[:, head_cols:],
        value_copy,
        output_copy,
    )


def solution(mesh):
    in_specs = (
        P("fs", "tp"),
        P("fs", "tp"),
        P("fs", "tp"),
        P("fs", "tp"),
        P("tp"),
        P(),
        P("fs", "tp"),
        P(),
        P(),
        P("fs", "tp"),
        P("tp", "fs"),
        P("fs", "tp"),
        P("fs", "tp"),
        P("fs", "tp"),
        P("fs", "tp"),
    )
    out_specs = (
        P("fs", "tp"),
        P("tp", "fs"),
        P("fs", "tp"),
        P("fs", "tp"),
        P("fs", "tp"),
        P("fs", "tp"),
        P(None, "tp"),
        P("tp", None),
    )
    return jax.shard_map(local, mesh=mesh, in_specs=in_specs, out_specs=out_specs, check_vma=False)
```

profile of v0, /device:TPU:2, one launch (start us, length us, event | category | flops | bytes accessed | tf_op | source)
XLA Modules:
  0.0 207.0 jit_solution(13290908280082833347)
XLA Ops:
  7.2 0.0 copy-start
  7.2 0.0 all-gather.3.cloned.1.call-start
  7.3 1.9 pad_maximum_fusion
  9.2 0.0 all-gather.3.cloned.1.call-update
  9.2 1.3 reshape.84
  10.5 0.3 reshape.85
  10.8 0.7 multiply_reduce_fusion
  11.5 0.1 broadcast_bitcast_fusion
  11.6 44.3 %all-gather.3.cloned.1.call-done = bf16[1024,2048]{1,0:T(8,128)(2,1)} async-done(((bf16[1024,256]{1,0:T(8,128)(2,1)}), bf16[1024,2048]{1,0:T(8,128)(2,1)}) %all-gather.3.cloned.1.call-update) | async-done | bytes 4194320 | tf_op jit(solution)/shard_map/all_gather | solution.py:15
  55.9 0.6 mul.124
  56.6 2.5 %convolution_multiply_fusion = f32[2048,256]{1,0:T(8,128)S(1)} fusion(bf16[1024,2048]{1,0:T(8,128)(2,1)} %all-gather.3.cloned.1.call-done, f32[64,8,2,128]{3,2,1,0:T(2,128)S(1)} %bitcast.25, f32[256]{0:T(256)S(1)} %get-tuple-element.43, f32[256]{0:T(256)S(1)} %get-tuple-element.44, bf16[512,256]{1,0:T(8,128)(2,1)S(1)} %copy-done.3, ...), kind=kOutput, calls=%fused_computation | convolution fusion | flops 538312704 | bytes 5244928 | tf_op jit(solution)/shard_map/dot_general | solution.py:64
  59.1 1.5 fusion.3
  60.7 2.3 %convolution_multiply_fusion.1 = f32[2048,256]{1,0:T(8,128)S(1)} fusion(bf16[512,256]{1,0:T(8,128)(2,1)S(1)} %copy-done.13, bf16[1024,2048]{1,0:T(8,128)(2,1)} %all-gather.3.cloned.1.call-done), kind=kOutput, calls=%fused_computation.1 | convolution fusion | flops 537395200 | bytes 4456448 | tf_op jit(solution)/shard_map/dot_general | solution.py:64
  63.1 1.5 fusion.2
  64.6 0.1 pad_maximum_fusion.1
  64.8 28.4 %all_to_all.10 = bf16[64,4,512]{2,1,0:T(4,128)(2,1)S(1)} all-to-all(bf16[64,4,512]{2,1,0:T(4,128)(2,1)S(1)} %pad_maximum_fusion.1), channel_id=1, replica_groups=mesh['fs'=64,'tp'=8] {'fs'}, dimensions={0} | all-to-all | bytes 524288 | tf_op jit(solution)/shard_map/all_to_all | solution.py:25
  93.2 0.1 convert_reduce_fusion
  93.4 0.9 broadcast_in_dim.2
  94.3 4.6 %all-to-all-start.1 = ((f32[64,4,512]{2,1,0:T(4,128)}), f32[64,4,512]{2,1,0:T(4,128)S(1)}, u32[]{:S(2)}, u32[]{:S(2)}) async-start(f32[64,4,512]{2,1,0:T(4,128)} %broadcast_in_dim.2), calls=%async_computation.1 | async-start | bytes 1048576 | tf_op jit(solution)/shard_map/all_to_all | solution.py:37
  98.9 0.0 all-gather.5.cloned.1.call-start
  98.9 18.6 %all-to-all-done.1 = f32[64,4,512]{2,1,0:T(4,128)S(1)} async-done(((f32[64,4,512]{2,1,0:T(4,128)}), f32[64,4,512]{2,1,0:T(4,128)S(1)}, u32[]{:S(2)}, u32[]{:S(2)}) %all-to-all-start.1) | async-done | bytes 524320 | tf_op jit(solution)/shard_map/all_to_all | solution.py:37
  117.5 0.2 reshape.86
  117.7 0.2 fusion.4
  118.0 0.0 copy-start.4
  118.0 0.9 fusion.25
  118.9 0.6 pad_maximum_fusion.2
  119.5 0.0 all-gather.5.cloned.1.call-update
  119.5 0.6 fusion.23
  120.1 0.6 fusion.24
  120.7 75.4 %all-gather.5.cloned.1.call-done = bf16[2048,512]{1,0:T(8,128)(2,1)} async-done(((bf16[32,512]{1,0:T(8,128)(2,1)}), bf16[2048,512]{1,0:T(8,128)(2,1)}) %all-gather.5.cloned.1.call-update) | async-done | bytes 2097168 | tf_op jit(solution)/shard_map/all_gather | solution.py:47
  196.1 2.6 %slice_bitcast_fusion = (bf16[256,2048]{0,1:T(8,128)(2,1)S(1)}, bf16[2048,256]{1,0:T(8,128)(2,1)}) fusion(bf16[2048,512]{1,0:T(8,128)(2,1)} %all-gather.5.cloned.1.call-done), kind=kLoop, calls=%fused_computation.12 | loop fusion | bytes 4194304 | tf_op jit(solution)/shard_map/transpose | solution.py:50
  198.8 1.4 copy.28
  (31 shorter events, 0.2 us)
Async XLA Ops:
  7.2 55.9 %copy-start = (bf16[2048,256]{1,0:T(8,128)(2,1)S(1)}, bf16[2048,256]{1,0:T(8,128)(2,1)}, u32[]{:S(2)}) copy-start(bf16[2048,256]{1,0:T(8,128)(2,1)} %param.22) | copy-start | bytes 3145732
  7.2 3.3 %copy-start.3 = (bf16[512,256]{1,0:T(8,128)(2,1)S(1)}, bf16[512,256]{1,0:T(8,128)(2,1)}, u32[]{:S(2)}) copy-start(bf16[512,256]{1,0:T(8,128)(2,1)} %param.18) | copy-start | bytes 786436
  7.2 3.6 %copy-start.11 = (f32[2]{0:T(128)S(1)}, f32[2]{0:T(128)}, u32[]{:S(2)}) copy-start(f32[2]{0:T(128)} %param.19) | copy-start | bytes 28
  7.2 4.3 %copy-start.12 = (f32[128]{0:T(128)S(1)}, f32[128]{0:T(128)}, u32[]{:S(2)}) copy-start(f32[128]{0:T(128)} %param.20) | copy-start | bytes 1540
  7.2 48.7 %all-gather.3.cloned.1.call-start = ((), (), s32[]{:S(2)}) async-start(), calls=%async_computation.2 | async-start | bytes 4718592 | tf_op jit(solution)/shard_map/all_gather | solution.py:15
  9.2 47.3 %copy-start.2 = (bf16[512,256]{1,0:T(8,128)(2,1)S(1)}, bf16[512,256]{1,0:T(8,128)(2,1)}, u32[]{:S(2)}) copy-start(bf16[512,256]{1,0:T(8,128)(2,1)} %param.17) | copy-start | bytes 786436
  56.6 2.5 %copy-start.1 = (bf16[2048,256]{1,0:T(8,128)(2,1)S(1)}, bf16[2048,256]{1,0:T(8,128)(2,1)}, u32[]{:S(2)}) copy-start(bf16[2048,256]{1,0:T(8,128)(2,1)} %param.23) | copy-start | bytes 3145732
  59.1 1.6 copy-start.13
  63.0 30.3 %copy-start.7 = (f32[4,256]{1,0:T(4,128)S(1)}, f32[4,256]{1,0:T(4,128)}, u32[]{:S(2)}) copy-start(f32[4,256]{1,0:T(4,128)} %param.29) | copy-start | bytes 12292
  63.0 30.3 %copy-start.8 = (f32[4,256]{1,0:T(4,128)S(1)}, f32[4,256]{1,0:T(4,128)}, u32[]{:S(2)}) copy-start(f32[4,256]{1,0:T(4,128)} %param.27) | copy-start | bytes 12292
  63.1 30.3 %copy-start.9 = (f32[4,256]{1,0:T(4,128)S(1)}, f32[4,256]{1,0:T(4,128)}, u32[]{:S(2)}) copy-start(f32[4,256]{1,0:T(4,128)} %param.28) | copy-start | bytes 12292
  63.1 30.3 %copy-start.10 = (f32[4,256]{1,0:T(4,128)S(1)}, f32[4,256]{1,0:T(4,128)}, u32[]{:S(2)}) copy-start(f32[4,256]{1,0:T(4,128)} %param.26) | copy-start | bytes 12292
  64.6 53.2 %copy-start.5 = (f32[256,32]{0,1:T(8,128)S(1)}, f32[256,32]{0,1:T(8,128)}, u32[]{:S(2)}) copy-start(f32[256,32]{0,1:T(8,128)} %param.25) | copy-start | bytes 98308
  64.6 53.4 %copy-start.6 = (f32[32,256]{1,0:T(8,128)S(1)}, f32[32,256]{1,0:T(8,128)}, u32[]{:S(2)}) copy-start(f32[32,256]{1,0:T(8,128)} %param.24) | copy-start | bytes 98308
  94.3 23.3 %all-to-all-start.1 = ((f32[64,4,512]{2,1,0:T(4,128)}), f32[64,4,512]{2,1,0:T(4,128)S(1)}, u32[]{:S(2)}, u32[]{:S(2)}) async-start(f32[64,4,512]{2,1,0:T(4,128)} %broadcast_in_dim.2), calls=%async_computation.1 | async-start | bytes 1048576 | tf_op jit(solution)/shard_map/all_to_all | solution.py:37
  98.9 97.2 %all-gather.5.cloned.1.call-start = ((), (), s32[]{:S(2)}) async-start(), calls=%async_computation.3 | async-start | bytes 2129920 | tf_op jit(solution)/shard_map/all_gather | solution.py:47
  118.0 80.8 %copy-start.4 = (f32[256,32]{0,1:T(8,128)}, f32[256,32]{0,1:T(8,128)S(1)}, u32[]{:S(2)}) copy-start(f32[256,32]{0,1:T(8,128)S(1)} %fusion.4) | copy-start | bytes 98308
Sparse Core Ops, SparseCore 0:
  10.7 45.1 all-gather.2
  119.6 76.4 all-gather.4
where the time goes:
time: 207 us
  waiting for transfers between devices  138 us (67%)
  blocking collectives  28.4 us (14%)
  between operations  14.3 us (7%)
  matrix products  8.94 us (4%)
  local copies, waits for them, and re-layouts  8.65 us (4%)
  starting transfers between devices  4.71 us (2%)
  other arithmetic  3.6 us (2%)
    all_gather x1, waiting for transfers between devices, gather_turned(): filled, at, done = (lax.all_gather(both, axis, axis=0, tiled=True), 0, [])  75.4 us
    all_gather x1, waiting for transfers between devices, side_by_side(): lax.all_gather(both, axis, axis=dim, tiled=True)  44.3 us
    all_to_all x1, blocking collectives, sum_at_owner(): tiles = lax.all_to_all(cut_along(x, dim, size), axis, 0, 0, tiled=True)  28.4 us
    all_to_all x1, waiting for transfers between devices, copy_for_each(): lax.all_to_all(jnp.broadcast_to(x[None], (size, *x.shape)), axis, 0, 0, t...  18.6 us
    dot_general x2, matrix products, contract_rows(): lax.dot_general(left, right, (((0,), (0,)), ((), ())), preferred_element_...  4.85 us
    all_to_all x1, starting transfers between devices, copy_for_each(): lax.all_to_all(jnp.broadcast_to(x[None], (size, *x.shape)), axis, 0, 0, t...  4.63 us
  transfers between devices with their start and end apart: 3, of which 3 were waited for; matrix products, arithmetic and copies ran while one was open for 2% of the time, Pallas kernels for 0%

commit v1 on v0

v1 whole, which is shorter than its diff:
```python
import math

import jax
import jax.numpy as jnp
from jax import lax
from jax.sharding import PartitionSpec as P

F32 = jnp.float32
BF16 = jnp.bfloat16
F16 = jnp.float16

WEIGHT_SCALE = 2.0**18
TOKEN_SCALE = 2.0**4
LOW_SCALE = 2.0**-2
DIRECTION_SCALE = 2.0**8


def dot(left, right, left_dim, right_dim):
    return lax.dot_general(
        left, right, (((left_dim,), (right_dim,)), ((), ())), preferred_element_type=F32
    )


def two_parts(x):
    high = lax.reduce_precision(x, 8, 7)
    return high.astype(BF16), (x - high).astype(BF16)


def dot_two(left, right_parts, left_dim, right_dim):
    high, low = right_parts
    return dot(left, high, left_dim, right_dim) + dot(left, low, left_dim, right_dim)


def copy_for_each(x, axis):
    size = lax.axis_size(axis)
    return lax.all_to_all(jnp.broadcast_to(x[None], (size, *x.shape)), axis, 0, 0, tiled=True)


def normed_heads(first_map, second_map, lambdas, head_gain):
    width = head_gain.shape[0]
    heads = []
    for h in range(lambdas.shape[0]):
        cols = slice(h * width, (h + 1) * width)
        difference = first_map[:, cols].astype(F32) - lambdas[h] * second_map[:, cols].astype(F32)
        mean = jnp.mean(difference * difference, axis=-1, keepdims=True)
        heads.append((difference * lax.rsqrt(mean + 1e-06) * head_gain[None, :]).astype(BF16))
    return jnp.concatenate(heads, axis=1)


def local(
    inputs,
    value_cotangent,
    first_map,
    second_map,
    lambdas,
    head_gain,
    output_cotangent,
    value_factor,
    output_factor,
    value_weight,
    output_weight,
    value_moment,
    value_second,
    output_moment,
    output_second,
):
    tok_rows, cols = inputs.shape
    rank = value_factor.shape[1]
    fs_size, tp_size = lax.axis_size("fs"), lax.axis_size("tp")
    fs_index, tp_index = lax.axis_index("fs"), lax.axis_index("tp")
    width_rows = value_weight.shape[0]

    own_weights = jnp.concatenate([value_weight, output_weight.T], axis=1)
    weights = lax.all_gather((own_weights * WEIGHT_SCALE).astype(F16), "fs", axis=0, tiled=True)

    in_rows = lax.dynamic_slice_in_dim(value_factor, tp_index * cols, cols, 0)
    cot_rows = lax.dynamic_slice_in_dim(output_factor, tp_index * cols, cols, 0)
    projected = jnp.concatenate(
        [dot(inputs, in_rows, 1, 0), dot(output_cotangent, cot_rows, 1, 0)], axis=1
    )
    pieces = (projected * TOKEN_SCALE).astype(F16).reshape(tp_size, -1, 2 * rank)
    pieces = lax.all_to_all(pieces, "tp", 0, 0, tiled=True)
    summed = jnp.sum(pieces.astype(F32), axis=0).astype(F16)
    tokens = copy_for_each(summed, "tp").reshape(tok_rows, 2 * rank).astype(F32)

    heads_out = normed_heads(first_map, second_map, lambdas, head_gain)
    scale = LOW_SCALE / (TOKEN_SCALE * math.sqrt(tok_rows * fs_size))
    token_parts = two_parts(tokens)
    low_value = dot_two(value_cotangent, [p[:, :rank] for p in token_parts], 0, 0)
    low_output = dot_two(heads_out, [p[:, rank:] for p in token_parts], 0, 0)
    partial = jnp.concatenate([low_value.T, low_output.T], axis=1) * scale
    tiles = partial.astype(F16).reshape(fs_size, -1, 2 * cols)
    tiles = lax.all_to_all(tiles, "fs", 0, 0, tiled=True)
    own_rows = jnp.sum(tiles.astype(F32), axis=0) * (1.0 / LOW_SCALE)

    moments = jnp.concatenate([value_moment, output_moment], axis=1)
    seconds = jnp.concatenate([value_second, output_second], axis=1)
    moment_new = 0.8 * moments + 0.2 * own_rows
    second_new = 0.95 * seconds + 0.05 * own_rows * own_rows
    direction = moment_new / (jnp.sqrt(second_new) + 1e-08)

    directions = copy_for_each((direction * DIRECTION_SCALE).astype(F16), "fs")
    parts = two_parts(directions.reshape(rank, 2 * cols).astype(F32))
    value_parts = [p[:, :cols] for p in parts]
    output_parts = [p[:, cols:] for p in parts]
    rate = 0.05 / DIRECTION_SCALE
    value_rows = lax.dynamic_slice_in_dim(value_factor, fs_index * width_rows, width_rows, 0)
    output_rows = lax.dynamic_slice_in_dim(output_factor, fs_index * width_rows, width_rows, 0)
    value_master = value_weight - rate * dot_two(value_rows, value_parts, 1, 0)
    output_master = output_weight - rate * dot_two(output_rows, output_parts, 1, 0).T

    old_value = weights[:, :cols].astype(F32) * (1.0 / WEIGHT_SCALE)
    old_output = weights[:, cols:].T.astype(F32) * (1.0 / WEIGHT_SCALE)
    value_copy = (old_value - rate * dot_two(value_factor, value_parts, 1, 0)).astype(BF16)
    step_output = dot(output_parts[0], output_factor, 0, 1) + dot(output_parts[1], output_factor, 0, 1)
    output_copy = (old_output - rate * step_output).astype(BF16)
    return (
        value_master,
        output_master,
        moment_new[:, :cols],
        second_new[:, :cols],
        moment_new[:, cols:],
        second_new[:, cols:],
        value_copy,
        output_copy,
    )


def solution(mesh):
    in_specs = (
        P("fs", "tp"),
        P("fs", "tp"),
        P("fs", "tp"),
        P("fs", "tp"),
        P("tp"),
        P(),
        P("fs", "tp"),
        P(),
        P(),
        P("fs", "tp"),
        P("tp", "fs"),
        P("fs", "tp"),
        P("fs", "tp"),
        P("fs", "tp"),
        P("fs", "tp"),
    )
    out_specs = (
        P("fs", "tp"),
        P("tp", "fs"),
        P("fs", "tp"),
        P("fs", "tp"),
        P("fs", "tp"),
        P("fs", "tp"),
        P(None, "tp"),
        P("tp", None),
    )
    return jax.shard_map(local, mesh=mesh, in_specs=in_specs, out_specs=out_specs, check_vma=False)
```

time: 207 us -> 145 us (0.70)
  the two profiles are of different devices: /device:TPU:2 before, /device:TPU:8 now
where the time goes in v1:
time: 145 us; the launch traced here: 144 us
  blocking collectives  52.9 us (36%)
  starting transfers between devices  35.1 us (24%)
  waiting for transfers between devices  22.7 us (16%)
  local copies, waits for them, and re-layouts  13.7 us (9%)
  matrix products  13.7 us (9%)
  other arithmetic  5.39 us (4%)
    all_gather x1, blocking collectives, local(): lax.all_gather((own_weights * WEIGHT_SCALE).astype(F16), 'fs', axis=0, ti...  52.9 us
    all_to_all x1, starting transfers between devices, local(): tiles = lax.all_to_all(tiles, 'fs', 0, 0, tiled=True)  16.6 us
    all_to_all x2, waiting for transfers between devices, copy_for_each(): lax.all_to_all(jnp.broadcast_to(x[None], (size, *x.shape)), axis, 0, 0, t...  14.5 us
    all_to_all x2, starting transfers between devices, copy_for_each(): lax.all_to_all(jnp.broadcast_to(x[None], (size, *x.shape)), axis, 0, 0, t...  14.1 us
    dot_general x14, matrix products, dot(): lax.dot_general(left, right, (((left_dim,), (right_dim,)), ((), ())), pre...  13.7 us
    all_to_all x1, waiting for transfers between devices, local(): pieces = lax.all_to_all(pieces, 'tp', 0, 0, tiled=True)  8.17 us
    unnamed x33, local copies, waits for them, and re-layouts  7.84 us
    all_to_all x1, starting transfers between devices, local(): pieces = lax.all_to_all(pieces, 'tp', 0, 0, tiled=True)  4.43 us
  transfers between devices with their start and end apart: 4, of which 3 were waited for; matrix products, arithmetic and copies ran while one was open for 8% of the time, Pallas kernels for 0%

profile of v1, /device:TPU:8, one launch (start us, length us, event | category | flops | bytes accessed | tf_op | source)
XLA Modules:
  0.0 144.4 jit_solution(10989713373295257813)
XLA Ops:
  0.7 1.2 copy-done
  1.9 1.2 convolution_bitcast_fusion.1
  3.3 1.2 convolution_bitcast_fusion
  4.7 0.9 fusion.12
  5.6 4.4 %all-to-all-start = ((f16[8,64,512]{2,1,0:T(8,128)(2,1)}), f16[8,64,512]{2,1,0:T(8,128)(2,1)S(1)}, u32[]{:S(2)}, u32[]{:S(2)}) async-start(f16[8,64,512]{2,1,0:T(8,128)(2,1)} %fusion.12), calls=%async_computation | async-start | bytes 1048576 | tf_op jit(solution)/shard_map/all_to_all | solution.py:82
  10.1 0.6 fusion.55
  10.7 1.5 %multiply_reduce_fusion.1 = (f32[512]{0:T(512)S(1)}, f32[512]{0:T(512)S(1)}) fusion(f32[]{:T(128)} %bitcast.6, bf16[512,256]{1,0:T(8,128)(2,1)S(1)} %copy-done.3, bf16[512,256]{1,0:T(8,128)(2,1)S(1)} %copy-done.4, f32[]{:T(128)} %bitcast.7), kind=kLoop, calls=%fused_computation.42 | loop fusion | flops 785408 | bytes 528392 | tf_op jit(solution)/shard_map/reduce_sum | solution.py:45
  12.2 8.2 %all-to-all-done = f16[8,64,512]{2,1,0:T(8,128)(2,1)S(1)} async-done(((f16[8,64,512]{2,1,0:T(8,128)(2,1)}), f16[8,64,512]{2,1,0:T(8,128)(2,1)S(1)}, u32[]{:S(2)}, u32[]{:S(2)}) %all-to-all-start) | async-done | bytes 524320 | tf_op jit(solution)/shard_map/all_to_all | solution.py:82
  20.5 0.8 broadcast_in_dim.4
  21.3 3.5 %all-to-all-start.1 = ((f16[8,64,512]{2,1,0:T(8,128)(2,1)}), f16[8,64,512]{2,1,0:T(8,128)(2,1)S(1)}, u32[]{:S(2)}, u32[]{:S(2)}) async-start(f16[8,64,512]{2,1,0:T(8,128)(2,1)} %broadcast_in_dim.4), calls=%async_computation.1 | async-start | bytes 1048576 | tf_op jit(solution)/shard_map/all_to_all | solution.py:36
  24.9 1.5 %multiply_convert_fusion.1 = (bf16[512,128]{1,0:T(8,128)(2,1)S(1)}, bf16[512,128]{1,0:T(8,128)(2,1)S(1)}) fusion(f32[128]{0:T(128)S(1)} %copy-done.14, f32[512]{0:T(512)S(1)} %get-tuple-element.52, f32[]{:T(128)} %bitcast.6, bf16[512,256]{1,0:T(8,128)(2,1)S(1)} %copy-done.3, bf16[512,256]{1,0:T(8,128)(2,1)S(1)} %copy-done.4, f32[512]{0:T(512)S(1)} %get-tuple-element.51, ...), kind=kLoop, calls=%fused_computation.41 | loop fusion | flops 917504 | bytes 791048 | tf_op jit(solution)/shard_map/convert_element_type | solution.py:46
  26.4 8.7 %all-to-all-done.1 = f16[8,64,512]{2,1,0:T(8,128)(2,1)S(1)} async-done(((f16[8,64,512]{2,1,0:T(8,128)(2,1)}), f16[8,64,512]{2,1,0:T(8,128)(2,1)S(1)}, u32[]{:S(2)}, u32[]{:S(2)}) %all-to-all-start.1) | async-done | bytes 524320 | tf_op jit(solution)/shard_map/all_to_all | solution.py:36
  35.3 0.3 fusion.16
  36.6 0.9 fusion.14
  37.4 16.6 %all-to-all-start.2 = ((f16[64,4,512]{2,1,0:T(4,128)(2,1)}), f16[64,4,512]{2,1,0:T(4,128)(2,1)S(1)}, u32[]{:S(2)}, u32[]{:S(2)}) async-start(f16[64,4,512]{2,1,0:T(4,128)(2,1)} %fusion.14), calls=%async_computation.2 | async-start | bytes 524288 | tf_op jit(solution)/shard_map/all_to_all | solution.py:93
  54.0 52.9 %all-gather.1 = f16[2048,512]{1,0:T(8,128)(2,1)S(1)} all-gather(f16[32,512]{1,0:T(8,128)(2,1)S(1)} %fusion.35), channel_id=1, replica_groups=mesh['fs'=64,'tp'=8] {'fs'}, dimensions={0}, use_global_device_ids=true | all-gather | bytes 2129920 | tf_op jit(solution)/shard_map/all_gather | solution.py:74
  107.1 0.8 broadcast_in_dim.5
  107.9 10.6 %all-to-all-start.3 = ((f16[64,4,512]{2,1,0:T(4,128)(2,1)}), f16[64,4,512]{2,1,0:T(4,128)(2,1)S(1)}, u32[]{:S(2)}, u32[]{:S(2)}) async-start(f16[64,4,512]{2,1,0:T(4,128)(2,1)} %broadcast_in_dim.5), calls=%async_computation.3 | async-start | bytes 524288 | tf_op jit(solution)/shard_map/all_to_all | solution.py:36
  118.5 1.8 %fusion.52 = (f16[2048,256]{1,0:T(8,128)(2,1)}, f16[2048,256]{1,0:T(8,128)(2,1)}) fusion(f16[2048,512]{1,0:T(8,128)(2,1)S(1)} %all-gather.1), kind=kLoop, calls=%fused_computation.80 | loop fusion | bytes 4194304 | tf_op jit(solution)/shard_map/slice | solution.py:113
  120.3 2.6 %copy.37 = f16[2048,256]{0,1:T(8,128)(2,1)} copy(f16[2048,256]{1,0:T(8,128)(2,1)} %get-tuple-element.37) | data formatting | bytes 2097152
  122.9 1.7 %copy.36 = f16[2048,256]{0,1:T(8,128)(2,1)} copy(f16[2048,256]{1,0:T(8,128)(2,1)S(1)} %copy-done.2) | data formatting | bytes 2097152
  124.6 0.6 fusion.53
  125.2 0.6 fusion.54
  125.8 5.8 %all-to-all-done.3 = f16[64,4,512]{2,1,0:T(4,128)(2,1)S(1)} async-done(((f16[64,4,512]{2,1,0:T(4,128)(2,1)}), f16[64,4,512]{2,1,0:T(4,128)(2,1)S(1)}, u32[]{:S(2)}, u32[]{:S(2)}) %all-to-all-start.3) | async-done | bytes 262176 | tf_op jit(solution)/shard_map/all_to_all | solution.py:36
  132.0 1.7 %fusion.25 = f32[256,2048]{1,0:T(8,128)S(1)} fusion(bf16[2048,256]{1,0:T(8,128)(2,1)} %param.23, bf16[256,512]{1,0:T(8,128)(2,1)S(1)} %get-tuple-element.42), kind=kOutput, calls=%fused_computation.48 | convolution fusion | flops 268435456 | bytes 3276800 | tf_op jit(solution)/shard_map/dot_general | solution.py:19
  133.7 0.5 fusion.31
  134.2 0.9 fusion.27
  135.2 1.6 %fusion.5 = bf16[2048,256]{0,1:T(8,128)(2,1)} fusion(f32[256,2048]{1,0:T(8,128)S(1)} %fusion.31, bf16[2048,256]{1,0:T(8,128)(2,1)S(1)} %copy-done, f16[2048,256]{0,1:T(8,128)(2,1)S(1)} %copy-done.1, bf16[256,512]{1,0:T(8,128)(2,1)S(1)} %get-tuple-element.41), kind=kOutput, calls=%fused_computation.7 | convolution fusion | flops 271581184 | bytes 5373952 | tf_op jit(solution)/shard_map/dot_general | solution.py:19
  136.8 2.3 %copy.35 = bf16[2048,256]{1,0:T(8,128)(2,1)} copy(bf16[2048,256]{0,1:T(8,128)(2,1)} %fusion.5) | data formatting | bytes 2097152
  139.1 1.5 %fusion.8 = f32[256,32]{0,1:T(8,128)} fusion(f32[256,32]{0,1:T(8,128)S(1)} %copy-done.7, f32[256,32]{0,1:T(8,128)S(1)} %fusion.27, bf16[256,512]{1,0:T(8,128)(2,1)S(1)} %get-tuple-element.41, bf16[2048,256]{1,0:T(8,128)(2,1)} %param.23, s32[]{:T(128)S(6)} %select_n.8), kind=kOutput, calls=%fused_computation.17 | convolution fusion | flops 4218880 | bytes 245764 | tf_op jit(solution)/shard_map/dot_general | solution.py:19
  140.6 0.8 fusion.10
  141.3 3.1 %fusion.6 = bf16[256,2048]{1,0:T(8,128)(2,1)} fusion(f32[256,2048]{1,0:T(8,128)S(1)} %fusion.25, bf16[2048,256]{1,0:T(8,128)(2,1)} %param.23, f16[2048,256]{0,1:T(8,128)(2,1)} %copy.37, bf16[256,512]{1,0:T(8,128)(2,1)S(1)} %get-tuple-element.41), kind=kOutput, calls=%fused_computation.8 | convolution fusion | flops 271581184 | bytes 5373952 | tf_op jit(solution)/shard_map/dot_general | solution.py:19
  (48 shorter events, 2.4 us)
Async XLA Ops:
  0.6 1.2 copy-start
  0.6 2.6 %copy-start.6 = (bf16[512,256]{1,0:T(8,128)(2,1)S(1)}, bf16[512,256]{1,0:T(8,128)(2,1)}, u32[]{:S(2)}) copy-start(bf16[512,256]{1,0:T(8,128)(2,1)} %param.21) | copy-start | bytes 786436
  3.3 6.8 %copy-start.13 = (f32[2]{0:T(128)S(1)}, f32[2]{0:T(128)}, u32[]{:S(2)}) copy-start(f32[2]{0:T(128)} %param.19) | copy-start | bytes 28
  3.3 7.4 %copy-start.7 = (f32[256,32]{0,1:T(8,128)S(1)}, f32[256,32]{0,1:T(8,128)}, u32[]{:S(2)}) copy-start(f32[256,32]{0,1:T(8,128)} %param.25) | copy-start | bytes 98308
  3.3 7.3 %copy-start.8 = (f32[32,256]{1,0:T(8,128)S(1)}, f32[32,256]{1,0:T(8,128)}, u32[]{:S(2)}) copy-start(f32[32,256]{1,0:T(8,128)} %param.24) | copy-start | bytes 98308
  4.5 6.2 %copy-start.3 = (bf16[512,256]{1,0:T(8,128)(2,1)S(1)}, bf16[512,256]{1,0:T(8,128)(2,1)}, u32[]{:S(2)}) copy-start(bf16[512,256]{1,0:T(8,128)(2,1)} %param.18) | copy-start | bytes 786436
  4.5 6.2 %copy-start.4 = (bf16[512,256]{1,0:T(8,128)(2,1)S(1)}, bf16[512,256]{1,0:T(8,128)(2,1)}, u32[]{:S(2)}) copy-start(bf16[512,256]{1,0:T(8,128)(2,1)} %param.17) | copy-start | bytes 786436
  5.6 19.2 %copy-start.14 = (f32[128]{0:T(128)S(1)}, f32[128]{0:T(128)}, u32[]{:S(2)}) copy-start(f32[128]{0:T(128)} %param.20) | copy-start | bytes 1540
  5.6 14.7 %all-to-all-start = ((f16[8,64,512]{2,1,0:T(8,128)(2,1)}), f16[8,64,512]{2,1,0:T(8,128)(2,1)S(1)}, u32[]{:S(2)}, u32[]{:S(2)}) async-start(f16[8,64,512]{2,1,0:T(8,128)(2,1)} %fusion.12), calls=%async_computation | async-start | bytes 1048576 | tf_op jit(solution)/shard_map/all_to_all | solution.py:82
  21.3 13.7 %all-to-all-start.1 = ((f16[8,64,512]{2,1,0:T(8,128)(2,1)}), f16[8,64,512]{2,1,0:T(8,128)(2,1)S(1)}, u32[]{:S(2)}, u32[]{:S(2)}) async-start(f16[8,64,512]{2,1,0:T(8,128)(2,1)} %broadcast_in_dim.4), calls=%async_computation.1 | async-start | bytes 1048576 | tf_op jit(solution)/shard_map/all_to_all | solution.py:36
  26.4 9.5 %copy-start.5 = (bf16[512,256]{1,0:T(8,128)(2,1)S(1)}, bf16[512,256]{1,0:T(8,128)(2,1)}, u32[]{:S(2)}) copy-start(bf16[512,256]{1,0:T(8,128)(2,1)} %param.16) | copy-start | bytes 786436
  36.4 70.6 %copy-start.9 = (f32[4,256]{1,0:T(4,128)S(1)}, f32[4,256]{1,0:T(4,128)}, u32[]{:S(2)}) copy-start(f32[4,256]{1,0:T(4,128)} %param.29) | copy-start | bytes 12292
  36.5 70.6 %copy-start.10 = (f32[4,256]{1,0:T(4,128)S(1)}, f32[4,256]{1,0:T(4,128)}, u32[]{:S(2)}) copy-start(f32[4,256]{1,0:T(4,128)} %param.27) | copy-start | bytes 12292
  36.5 70.6 %copy-start.11 = (f32[4,256]{1,0:T(4,128)S(1)}, f32[4,256]{1,0:T(4,128)}, u32[]{:S(2)}) copy-start(f32[4,256]{1,0:T(4,128)} %param.28) | copy-start | bytes 12292
  36.5 70.6 %copy-start.12 = (f32[4,256]{1,0:T(4,128)S(1)}, f32[4,256]{1,0:T(4,128)}, u32[]{:S(2)}) copy-start(f32[4,256]{1,0:T(4,128)} %param.26) | copy-start | bytes 12292
  37.4 69.5 %all-to-all-start.2 = ((f16[64,4,512]{2,1,0:T(4,128)(2,1)}), f16[64,4,512]{2,1,0:T(4,128)(2,1)S(1)}, u32[]{:S(2)}, u32[]{:S(2)}) async-start(f16[64,4,512]{2,1,0:T(4,128)(2,1)} %fusion.14), calls=%async_computation.2 | async-start | bytes 524288 | tf_op jit(solution)/shard_map/all_to_all | solution.py:93
  107.9 23.7 %all-to-all-start.3 = ((f16[64,4,512]{2,1,0:T(4,128)(2,1)}), f16[64,4,512]{2,1,0:T(4,128)(2,1)S(1)}, u32[]{:S(2)}, u32[]{:S(2)}) async-start(f16[64,4,512]{2,1,0:T(4,128)(2,1)} %broadcast_in_dim.5), calls=%async_computation.3 | async-start | bytes 524288 | tf_op jit(solution)/shard_map/all_to_all | solution.py:36
  120.3 2.6 %copy-start.2 = (f16[2048,256]{1,0:T(8,128)(2,1)S(1)}, f16[2048,256]{1,0:T(8,128)(2,1)}, u32[]{:S(2)}) copy-start(f16[2048,256]{1,0:T(8,128)(2,1)} %get-tuple-element.38) | copy-start | bytes 3145732
  133.7 1.5 %copy-start.1 = (f16[2048,256]{0,1:T(8,128)(2,1)S(1)}, f16[2048,256]{0,1:T(8,128)(2,1)}, u32[]{:S(2)}) copy-start(f16[2048,256]{0,1:T(8,128)(2,1)} %copy.36) | copy-start | bytes 3145732

commit v2 on v1

v2 whole, which is shorter than its diff:
```python
import math

import jax
import jax.numpy as jnp
from jax import lax
from jax.experimental import pallas as pl
from jax.experimental.pallas import tpu as pltpu
from jax.sharding import Mesh, PartitionSpec as P

F32 = jnp.float32
BF16 = jnp.bfloat16
F16 = jnp.float16

FS = ("z", "y")
TP = ("x", "core")

WEIGHT_SCALE = 2.0**18
TOKEN_SCALE = 2.0**4
LOW_SCALE = 2.0**-2
DIRECTION_SCALE = 2.0**8

GROUP = 512


def dot(left, right, left_dim, right_dim):
    return lax.dot_general(
        left, right, (((left_dim,), (right_dim,)), ((), ())), preferred_element_type=F32
    )


def two_parts(x):
    high = lax.reduce_precision(x, 8, 7)
    return high.astype(BF16), (x - high).astype(BF16)


def dot_two(left, right_parts, left_dim, right_dim):
    high, low = right_parts
    return dot(left, high, left_dim, right_dim) + dot(left, low, left_dim, right_dim)


def copy_for_each(x, axis):
    size = lax.axis_size(axis)
    return lax.all_to_all(jnp.broadcast_to(x[None], (size, *x.shape)), axis, 0, 0, tiled=True)


def normed_heads(first_map, second_map, lambdas, head_gain):
    width = head_gain.shape[0]
    heads = []
    for h in range(lambdas.shape[0]):
        cols = slice(h * width, (h + 1) * width)
        difference = first_map[:, cols].astype(F32) - lambdas[h] * second_map[:, cols].astype(F32)
        mean = jnp.mean(difference * difference, axis=-1, keepdims=True)
        heads.append((difference * lax.rsqrt(mean + 1e-06) * head_gain[None, :]).astype(BF16))
    return jnp.concatenate(heads, axis=1)


def from_offset(x, dy, dz):
    ny, nz = lax.axis_size("y"), lax.axis_size("z")
    pairs = []
    for z in range(nz):
        for y in range(ny):
            source = ((z + dz) % nz) * ny + (y + dy) % ny
            pairs.append((source, z * ny + y))
    return lax.ppermute(x, FS, pairs)


DOUBLINGS = ((4, 0), (0, 4), (0, 2), (2, 1))
NEIGHBOURS = ((1, 0), (0, 1), (-1, 0))


def gathered_blocks(block):
    ny, nz = lax.axis_size("y"), lax.axis_size("z")
    held, offsets = block[None], [(0, 0)]
    for dy, dz in DOUBLINGS:
        held = jnp.concatenate([held, from_offset(held, dy, dz)], axis=0)
        offsets = offsets + [(y + dy, z + dz) for y, z in offsets]
    quarters, base = [held], list(offsets)
    for dy, dz in NEIGHBOURS:
        quarters.append(from_offset(held, dy, dz))
        offsets = offsets + [(y + dy, z + dz) for y, z in base]
    place = {(y % ny, z % nz): slot for slot, (y, z) in enumerate(offsets)}
    table = jnp.array([[place[y, z] for y in range(ny)] for z in range(nz)], jnp.int32)
    zs = (jnp.arange(nz) - lax.axis_index("z")) % nz
    ys = (jnp.arange(ny) - lax.axis_index("y")) % ny
    slots = table[zs[:, None], ys[None, :]].reshape(-1)
    return jnp.concatenate(quarters, axis=0), slots


def last_kernel(
    slots,
    blocks,
    high,
    low,
    value_factor,
    output_factor,
    own_value_factor,
    own_output_factor,
    value_weight,
    output_weight_t,
    value_copy,
    output_copy,
    value_master,
    output_master_t,
    high_t,
    low_t,
):
    step = pl.program_id(0)
    cols = value_copy.shape[1]
    width_rows = blocks.shape[1]
    rate = 0.05 / DIRECTION_SCALE

    @pl.when(step == 0)
    def _():
        high_t[...] = high[:, cols:].T
        low_t[...] = low[:, cols:].T
        value_master[...] = value_weight[...] - rate * (
            dot(own_value_factor[...], high[:, :cols], 1, 0)
            + dot(own_value_factor[...], low[:, :cols], 1, 0)
        )
        output_master_t[...] = output_weight_t[...] - rate * (
            dot(own_output_factor[...], high_t[...], 1, 1)
            + dot(own_output_factor[...], low_t[...], 1, 1)
        )

    per_step = value_copy.shape[0] // width_rows
    old = jnp.concatenate(
        [blocks[slots[step * per_step + i]] for i in range(per_step)], axis=0
    ) * (1.0 / WEIGHT_SCALE)
    value_step = dot(value_factor[...], high[:, :cols], 1, 0) + dot(
        value_factor[...], low[:, :cols], 1, 0
    )
    value_copy[...] = (old[:, :cols] - rate * value_step).astype(BF16)
    output_step = dot(high_t[...], output_factor[...], 1, 1) + dot(
        low_t[...], output_factor[...], 1, 1
    )
    output_copy[...] = (old[:, cols:].T - rate * output_step).astype(BF16)


def last_step(slots, blocks, high, low, value_factor, output_factor, own_v, own_o, value_weight, output_weight_t):
    width, rank = value_factor.shape
    rows, cols = value_weight.shape
    whole = lambda *shape: pl.BlockSpec(shape, lambda i, s: (0,) * len(shape))
    return pl.pallas_call(
        last_kernel,
        grid_spec=pltpu.PrefetchScalarGridSpec(
            num_scalar_prefetch=1,
            grid=(width // GROUP,),
            in_specs=[
                whole(*blocks.shape),
                whole(*high.shape),
                whole(*low.shape),
                pl.BlockSpec((GROUP, rank), lambda i, s: (i, 0)),
                pl.BlockSpec((GROUP, rank), lambda i, s: (i, 0)),
                whole(*own_v.shape),
                whole(*own_o.shape),
                whole(rows, cols),
                whole(rows, cols),
            ],
            out_specs=[
                pl.BlockSpec((GROUP, cols), lambda i, s: (i, 0)),
                pl.BlockSpec((cols, GROUP), lambda i, s: (0, i)),
                whole(rows, cols),
                whole(rows, cols),
            ],
            scratch_shapes=[
                pltpu.VMEM((cols, rank), BF16),
                pltpu.VMEM((cols, rank), BF16),
            ],
        ),
        out_shape=[
            jax.ShapeDtypeStruct((width, cols), BF16),
            jax.ShapeDtypeStruct((cols, width), BF16),
            jax.ShapeDtypeStruct((rows, cols), F32),
            jax.ShapeDtypeStruct((rows, cols), F32),
        ],
        name="last_step",
    )(slots, blocks, high, low, value_factor, output_factor, own_v, own_o, value_weight, output_weight_t)


def local(
    inputs,
    value_cotangent,
    first_map,
    second_map,
    lambdas,
    head_gain,
    output_cotangent,
    value_factor,
    output_factor,
    value_weight,
    output_weight,
    value_moment,
    value_second,
    output_moment,
    output_second,
):
    tok_rows, cols = inputs.shape
    rank = value_factor.shape[1]
    fs_size, tp_size = lax.axis_size(FS), lax.axis_size(TP)
    fs_index, tp_index = lax.axis_index(FS), lax.axis_index(TP)
    width_rows = value_weight.shape[0]

    output_weight_t = output_weight.T
    own_weights = jnp.concatenate([value_weight, output_weight_t], axis=1)
    with jax.named_scope("weights"):
        blocks, slots = gathered_blocks((own_weights * WEIGHT_SCALE).astype(F16))

    in_rows = lax.dynamic_slice_in_dim(value_factor, tp_index * cols, cols, 0)
    cot_rows = lax.dynamic_slice_in_dim(output_factor, tp_index * cols, cols, 0)
    projected = jnp.concatenate(
        [dot(inputs, in_rows, 1, 0), dot(output_cotangent, cot_rows, 1, 0)], axis=1
    )
    pieces = (projected * TOKEN_SCALE).astype(F16).reshape(tp_size, -1, 2 * rank)
    pieces = lax.all_to_all(pieces, TP, 0, 0, tiled=True)
    summed = jnp.sum(pieces.astype(F32), axis=0).astype(F16)
    tokens = copy_for_each(summed, TP).reshape(tok_rows, 2 * rank).astype(F32)

    heads_out = normed_heads(first_map, second_map, lambdas, head_gain)
    scale = LOW_SCALE / (TOKEN_SCALE * math.sqrt(tok_rows * fs_size))
    token_parts = two_parts(tokens)
    low_value = dot_two(value_cotangent, [p[:, :rank] for p in token_parts], 0, 0)
    low_output = dot_two(heads_out, [p[:, rank:] for p in token_parts], 0, 0)
    partial = jnp.concatenate([low_value.T, low_output.T], axis=1) * scale
    tiles = partial.astype(F16).reshape(fs_size, -1, 2 * cols)
    tiles = lax.all_to_all(tiles, FS, 0, 0, tiled=True)
    own_rows = jnp.sum(tiles.astype(F32), axis=0) * (1.0 / LOW_SCALE)

    moments = jnp.concatenate([value_moment, output_moment], axis=1)
    seconds = jnp.concatenate([value_second, output_second], axis=1)
    moment_new = 0.8 * moments + 0.2 * own_rows
    second_new = 0.95 * seconds + 0.05 * own_rows * own_rows
    direction = moment_new / (jnp.sqrt(second_new) + 1e-08)

    directions = copy_for_each((direction * DIRECTION_SCALE).astype(F16), FS)
    high, low = two_parts(directions.astype(F32).reshape(rank, 2 * cols))
    own_v = lax.dynamic_slice_in_dim(value_factor, fs_index * width_rows, width_rows, 0)
    own_o = lax.dynamic_slice_in_dim(output_factor, fs_index * width_rows, width_rows, 0)
    value_copy, output_copy, value_master, output_master_t = last_step(
        slots, blocks.astype(F32), high, low, value_factor, output_factor, own_v, own_o, value_weight, output_weight_t
    )
    return (
        value_master,
        output_master_t.T,
        moment_new[:, :cols],
        second_new[:, :cols],
        moment_new[:, cols:],
        second_new[:, cols:],
        value_copy,
        output_copy,
    )


def solution(mesh):
    fs, tp = mesh.devices.shape
    fine = Mesh(mesh.devices.reshape(8, fs // 8, tp // 2, 2), (*FS, *TP))
    rows_cols = P(FS, TP)
    in_specs = (rows_cols,) * 4 + (P(TP), P(), rows_cols, P(), P(), rows_cols, P(TP, FS)) + (rows_cols,) * 4
    out_specs = (rows_cols, P(TP, FS)) + (rows_cols,) * 4 + (P(None, TP), P(TP, None))
    return jax.shard_map(local, mesh=fine, in_specs=in_specs, out_specs=out_specs, check_vma=False)
```

time: 145 us -> 131 us (0.903)
  blocking collectives: 52.9 us -> 0 us
  starting transfers between devices: 35.1 us -> 69.4 us
  matrix products: 13.7 us -> 3.4 us
  Pallas kernels: 0 us -> 6.99 us
  other arithmetic: 5.39 us -> 10.9 us
  waiting for transfers between devices: 22.7 us -> 24.9 us
    all_gather x1 -> x0, blocking collectives: 52.9 us -> none  [local(): lax.all_gather((own_weights * WEIGHT_SCALE).astype(F16), 'fs', axis=0, ti...]
    ppermute x0 -> x7, starting transfers between devices: none -> 44.1 us  [from_offset(): return lax.ppermute(x, FS, pairs)]
    ppermute x0 -> x7, waiting for transfers between devices: none -> 10.7 us  [from_offset(): return lax.ppermute(x, FS, pairs)]
    dot_general x14 -> x6, matrix products: 13.7 us -> 3.4 us  [dot(): lax.dot_general(left, right, (((left_dim,), (right_dim,)), ((), ())), pre...]
    pallas_call x0 -> x1, Pallas kernels: none -> 6.99 us  [last_step(): pl.pallas_call(last_kernel, grid_spec=pltpu.PrefetchScalarGridSpec(num_sc...]
    all_to_all x2, starting transfers between devices: 21 us -> 14.1 us  [the longest x1 9.83 us: local(): tiles = lax.all_to_all(tiles, FS, 0, 0, tiled=True)]
    all_to_all x2, waiting for transfers between devices: 14.5 us -> 9.22 us  [copy_for_each(): lax.all_to_all(jnp.broadcast_to(x[None], (size, *x.shape)), axis, 0, 0, t...]
    all_to_all x2, waiting for transfers between devices: 8.17 us -> 5.01 us  [the longest x1 5.01 us: local(): tiles = lax.all_to_all(tiles, FS, 0, 0, tiled=True)]
  transfers between devices with their start and end apart: 4 -> 11, of which waited for: 3 -> 6; matrix products, arithmetic and copies ran while one was open for 8% -> 17% of each run, Pallas kernels for 0% -> 0%
where the time goes in v2:
time: 131 us; the launch traced here: 130 us
  starting transfers between devices  69.4 us (53%)
  waiting for transfers between devices  24.9 us (19%)
  local copies, waits for them, and re-layouts  13.9 us (11%)
  other arithmetic  10.9 us (8%)
  Pallas kernels  6.99 us (5%)
  matrix products  3.4 us (3%)
    ppermute x7, starting transfers between devices, from_offset(): return lax.ppermute(x, FS, pairs)  44.1 us
    all_to_all x2, starting transfers between devices, copy_for_each(): lax.all_to_all(jnp.broadcast_to(x[None], (size, *x.shape)), axis, 0, 0, t...  11.2 us
    ppermute x7, waiting for transfers between devices, from_offset(): return lax.ppermute(x, FS, pairs)  10.7 us
    all_to_all x1, starting transfers between devices, local(): tiles = lax.all_to_all(tiles, FS, 0, 0, tiled=True)  9.83 us
    all_to_all x2, waiting for transfers between devices, copy_for_each(): lax.all_to_all(jnp.broadcast_to(x[None], (size, *x.shape)), axis, 0, 0, t...  9.22 us
    pallas_call x1, Pallas kernels, last_step(): pl.pallas_call(last_kernel, grid_spec=pltpu.PrefetchScalarGridSpec(num_sc...  6.99 us
    unnamed x36, local copies, waits for them, and re-layouts  5.25 us
    all_to_all x1, waiting for transfers between devices, local(): tiles = lax.all_to_all(tiles, FS, 0, 0, tiled=True)  5.01 us
  transfers between devices with their start and end apart: 11, of which 6 were waited for; matrix products, arithmetic and copies ran while one was open for 17% of the time, Pallas kernels for 0%

profile of v2, /device:TPU:8, one launch (start us, length us, event | category | flops | bytes accessed | tf_op | source)
XLA Modules:
  0.0 130.5 jit_solution(7603218046205716869)
XLA Ops:
  0.7 0.9 copy-done
  1.6 1.2 convolution_bitcast_fusion.1
  3.0 1.2 convolution_bitcast_fusion
  4.4 0.9 fusion.1
  5.3 4.3 %all-to-all-start = ((f16[8,64,512]{2,1,0:T(8,128)(2,1)}), f16[8,64,512]{2,1,0:T(8,128)(2,1)S(1)}, u32[]{:S(2)}, u32[]{:S(2)}) async-start(f16[8,64,512]{2,1,0:T(8,128)(2,1)} %fusion.1), calls=%async_computation | async-start | bytes 1048576 | tf_op jit(solution)/shard_map/all_to_all | solution.py:214
  10.3 6.8 %collective-permute-start = (f16[1,32,512]{2,1,0:T(8,128)(2,1)S(1)}, f16[1,32,512]{2,1,0:T(8,128)(2,1)S(1)}, u32[]{:S(2)}, u32[]{:S(2)}) collective-permute-start(f16[1,32,512]{2,1,0:T(8,128)(2,1)S(1)} %get-tuple-element.22), channel_id=1, source_target_pairs={{32,0},{40,8},{48,16},{56,24},{0,32},{8,40},{16,48},{24,56},{96,64... | collective-permute-start | bytes 98312 | tf_op jit(solution)/shard_map/weights/ppermute | solution.py:64
  17.7 1.5 %multiply_reduce_fusion.1 = (f32[512]{0:T(512)S(1)}, f32[512]{0:T(512)S(1)}) fusion(f32[]{:T(128)} %bitcast.9, bf16[512,256]{1,0:T(8,128)(2,1)S(1)} %copy-done.2, bf16[512,256]{1,0:T(8,128)(2,1)S(1)} %copy-done.3, f32[]{:T(128)} %bitcast.10), kind=kLoop, calls=%fused_computation.29 | loop fusion | flops 785408 | bytes 528392 | tf_op jit(solution)/shard_map/reduce_sum | solution.py:52
  20.0 10.9 %collective-permute-start.1 = (f16[2,32,512]{2,1,0:T(8,128)(2,1)S(1)}, f16[2,32,512]{2,1,0:T(8,128)(2,1)S(1)}, u32[]{:S(2)}, u32[]{:S(2)}) collective-permute-start(f16[2,32,512]{2,1,0:T(8,128)(2,1)S(1)} %pad_maximum_fusion.5), channel_id=1, source_target_pairs={{256,0},{264,8},{272,16},{280,24},{288,32},{296,40},{304,48},{312,... | collective-permute-start | bytes 196616 | tf_op jit(solution)/shard_map/weights/ppermute | solution.py:64
  30.9 2.1 %multiply_convert_fusion.1 = (bf16[512,128]{1,0:T(8,128)(2,1)S(1)}, bf16[512,128]{1,0:T(8,128)(2,1)}) fusion(f32[128]{0:T(128)S(1)} %copy-done.14, f32[512]{0:T(512)S(1)} %get-tuple-element.46, f32[]{:T(128)} %bitcast.9, bf16[512,256]{1,0:T(8,128)(2,1)S(1)} %copy-done.2, bf16[512,256]{1,0:T(8,128)(2,1)S(1)} %copy-done.3, f32[512]{0:T(512)S(1)} %get-tuple-element.45, ...), kind=kLoop, calls=%fused_computation.28 | loop fusion | flops 917504 | bytes 791048 | tf_op jit(solution)/shard_map/convert_element_type | solution.py:53
  33.7 7.6 %collective-permute-start.2 = (f16[4,32,512]{2,1,0:T(8,128)(2,1)S(1)}, f16[4,32,512]{2,1,0:T(8,128)(2,1)S(1)}, u32[]{:S(2)}, u32[]{:S(2)}) collective-permute-start(f16[4,32,512]{2,1,0:T(8,128)(2,1)S(1)} %pad_maximum_fusion.4), channel_id=1, source_target_pairs={{128,0},{136,8},{144,16},{152,24},{160,32},{168,40},{176,48},{184,... | collective-permute-start | bytes 393224 | tf_op jit(solution)/shard_map/weights/ppermute | solution.py:64
  41.3 4.5 %collective-permute-done.2 = f16[4,32,512]{2,1,0:T(8,128)(2,1)S(1)} collective-permute-done((f16[4,32,512]{2,1,0:T(8,128)(2,1)S(1)}, f16[4,32,512]{2,1,0:T(8,128)(2,1)S(1)}, u32[]{:S(2)}, u32[]{:S(2)}) %collective-permute-start.2) | collective-permute-done | bytes 131104 | tf_op jit(solution)/shard_map/weights/ppermute | solution.py:64
  46.6 9.5 %collective-permute-start.3 = (f16[8,32,512]{2,1,0:T(8,128)(2,1)}, f16[8,32,512]{2,1,0:T(8,128)(2,1)}, u32[]{:S(2)}, u32[]{:S(2)}) collective-permute-start(f16[8,32,512]{2,1,0:T(8,128)(2,1)} %pad_maximum_fusion), channel_id=1, source_target_pairs={{80,0},{88,8},{96,16},{104,24},{112,32},{120,40},{64,48},{72,56},{... | collective-permute-start | bytes 786440 | tf_op jit(solution)/shard_map/weights/ppermute | solution.py:64
  56.2 0.8 broadcast_in_dim.10
  57.0 3.6 %all-to-all-start.1 = ((f16[8,64,512]{2,1,0:T(8,128)(2,1)}), f16[8,64,512]{2,1,0:T(8,128)(2,1)S(1)}, u32[]{:S(2)}, u32[]{:S(2)}) async-start(f16[8,64,512]{2,1,0:T(8,128)(2,1)} %broadcast_in_dim.10), calls=%async_computation.1 | async-start | bytes 1048576 | tf_op jit(solution)/shard_map/all_to_all | solution.py:43
  62.6 4.9 %collective-permute-done.3 = f16[8,32,512]{2,1,0:T(8,128)(2,1)} collective-permute-done((f16[8,32,512]{2,1,0:T(8,128)(2,1)}, f16[8,32,512]{2,1,0:T(8,128)(2,1)}, u32[]{:S(2)}, u32[]{:S(2)}) %collective-permute-start.3) | collective-permute-done | bytes 262176 | tf_op jit(solution)/shard_map/weights/ppermute | solution.py:64
  67.5 1.7 %constant_dynamic-update-slice_fusion = (f16[16,32,512]{2,1,0:T(8,128)(2,1)}, f16[64,32,512]{2,1,0:T(8,128)(2,1)S(1)}) fusion(f16[16,32,512]{2,1,0:T(8,128)(2,1)} %get-tuple-element.31, f16[8,32,512]{2,1,0:T(8,128)(2,1)} %collective-permute-done.3, f16[64,32,512]{2,1,0:T(8,128)(2,1)S(1)} %get-tuple-element.32), kind=kLoop, calls=%fused_computation.37 | loop fusion | bytes 786432 | tf_op jit(solution)/shard_map/weights/concatenate | solution.py:75
  69.2 1.9 %collective-permute-start.5 = (f16[16,32,512]{2,1,0:T(8,128)(2,1)}, f16[16,32,512]{2,1,0:T(8,128)(2,1)}, u32[]{:S(2)}, u32[]{:S(2)}) collective-permute-start(f16[16,32,512]{2,1,0:T(8,128)(2,1)} %get-tuple-element.29), channel_id=1, source_target_pairs={{64,0},{72,8},{80,16},{88,24},{96,32},{104,40},{112,48},{120,56},{... | collective-permute-start | bytes 1572872 | tf_op jit(solution)/shard_map/weights/ppermute | solution.py:64
  71.1 4.0 %collective-permute-start.4 = (f16[16,32,512]{2,1,0:T(8,128)(2,1)}, f16[16,32,512]{2,1,0:T(8,128)(2,1)}, u32[]{:S(2)}, u32[]{:S(2)}) collective-permute-start(f16[16,32,512]{2,1,0:T(8,128)(2,1)} %get-tuple-element.29), channel_id=1, source_target_pairs={{8,0},{16,8},{24,16},{32,24},{40,32},{48,40},{56,48},{0,56},{72,64... | collective-permute-start | bytes 1572872 | tf_op jit(solution)/shard_map/weights/ppermute | solution.py:64
  76.6 0.9 fusion.3
  77.5 9.8 %all-to-all-start.2 = ((f16[64,4,512]{2,1,0:T(4,128)(2,1)}), f16[64,4,512]{2,1,0:T(4,128)(2,1)S(1)}, u32[]{:S(2)}, u32[]{:S(2)}) async-start(f16[64,4,512]{2,1,0:T(4,128)(2,1)} %fusion.3), calls=%async_computation.2 | async-start | bytes 524288 | tf_op jit(solution)/shard_map/all_to_all | solution.py:225
  87.4 1.2 gather_fusion
  88.7 1.4 %constant_dynamic-slice_fusion = (bf16[32,256]{1,0:T(8,128)(2,1)}, bf16[32,256]{1,0:T(8,128)(2,1)}) fusion(bf16[2048,256]{1,0:T(8,128)(2,1)} %output_factor.1, s32[]{:T(128)S(6)} %select_n.46, bf16[2048,256]{1,0:T(8,128)(2,1)} %value_factor.1), kind=kLoop, calls=%fused_computation.67 | loop fusion | bytes 65540 | tf_op jit(solution)/shard_map/dynamic_slice | solution.py:237
  90.1 3.4 %collective-permute-start.6 = (f16[16,32,512]{2,1,0:T(8,128)(2,1)}, f16[16,32,512]{2,1,0:T(8,128)(2,1)S(1)}, u32[]{:S(2)}, u32[]{:S(2)}) collective-permute-start(f16[16,32,512]{2,1,0:T(8,128)(2,1)} %get-tuple-element.29), channel_id=1, source_target_pairs={{56,0},{0,8},{8,16},{16,24},{24,32},{32,40},{40,48},{48,56},{120,6... | collective-permute-start | bytes 1572872 | tf_op jit(solution)/shard_map/weights/ppermute | solution.py:64
  93.5 1.1 constant_dynamic-update-slice_fusion.7
  94.6 1.1 constant_dynamic-update-slice_fusion.6
  95.8 5.0 %all-to-all-done.2 = f16[64,4,512]{2,1,0:T(4,128)(2,1)S(1)} async-done(((f16[64,4,512]{2,1,0:T(4,128)(2,1)}), f16[64,4,512]{2,1,0:T(4,128)(2,1)S(1)}, u32[]{:S(2)}, u32[]{:S(2)}) %all-to-all-start.2) | async-done | bytes 262176 | tf_op jit(solution)/shard_map/all_to_all | solution.py:225
  101.0 0.8 broadcast_in_dim.11
  101.8 7.5 %all-to-all-start.3 = ((f16[64,4,512]{2,1,0:T(4,128)(2,1)}), f16[64,4,512]{2,1,0:T(4,128)(2,1)S(1)}, u32[]{:S(2)}, u32[]{:S(2)}) async-start(f16[64,4,512]{2,1,0:T(4,128)(2,1)} %broadcast_in_dim.11), calls=%async_computation.3 | async-start | bytes 524288 | tf_op jit(solution)/shard_map/all_to_all | solution.py:43
  109.4 2.5 %convert_element_type.79.blocks = f32[64,32,512]{2,1,0:T(8,128)} convert(f16[64,32,512]{2,1,0:T(8,128)(2,1)S(1)} %constant_dynamic-update-slice_fusion.5) | non-fusion elementwise | flops 1048576 | bytes 6291456 | tf_op jit(solution)/shard_map/convert_element_type | solution.py:239
  113.1 9.2 %all-to-all-done.3 = f16[64,4,512]{2,1,0:T(4,128)(2,1)S(1)} async-done(((f16[64,4,512]{2,1,0:T(4,128)(2,1)}), f16[64,4,512]{2,1,0:T(4,128)(2,1)S(1)}, u32[]{:S(2)}, u32[]{:S(2)}) %all-to-all-start.3) | async-done | bytes 262176 | tf_op jit(solution)/shard_map/all_to_all | solution.py:43
  122.6 0.9 fusion.2
  123.5 7.0 %last_step.1 = (bf16[2048,256]{1,0:T(8,128)(2,1)}, bf16[256,2048]{1,0:T(8,128)(2,1)}, f32[32,256]{1,0:T(8,128)}, f32[32,256]{1,0:T(8,128)}) custom-call(s32[64]{0:T(128)} %gather_fusion, f32[64,32,512]{2,1,0:T(8,128)} %convert_element_type.79.blocks, bf16[256,512]{1,0:T(8,128)(2,1)} %get-tuple-element.26.high, bf16[256,512]{1,0:T(8,128)(2,1)} %get-tuple-element.25.low, ...), custom_call_target="tpu_custom_call" | custom-call | tf_op jit(solution)/shard_map/last_step/pallas_call | solution.py:143
  (67 shorter events, 9.2 us)
Async XLA Ops:
  0.6 1.0 copy-start
  0.6 2.3 %copy-start.5 = (bf16[512,256]{1,0:T(8,128)(2,1)S(1)}, bf16[512,256]{1,0:T(8,128)(2,1)}, u32[]{:S(2)}) copy-start(bf16[512,256]{1,0:T(8,128)(2,1)} %param.22) | copy-start | bytes 786436
  3.0 6.6 %copy-start.6 = (f32[256,32]{0,1:T(8,128)S(1)}, f32[256,32]{0,1:T(8,128)}, u32[]{:S(2)}) copy-start(f32[256,32]{0,1:T(8,128)} %param.26) | copy-start | bytes 98308
  3.0 6.6 %copy-start.7 = (f32[32,256]{1,0:T(8,128)S(1)}, f32[32,256]{1,0:T(8,128)}, u32[]{:S(2)}) copy-start(f32[32,256]{1,0:T(8,128)} %value_weight.1) | copy-start | bytes 98308
  4.2 12.9 %copy-start.13 = (f32[2]{0:T(128)S(1)}, f32[2]{0:T(128)}, u32[]{:S(2)}) copy-start(f32[2]{0:T(128)} %param.20) | copy-start | bytes 28
  4.2 13.5 %copy-start.2 = (bf16[512,256]{1,0:T(8,128)(2,1)S(1)}, bf16[512,256]{1,0:T(8,128)(2,1)}, u32[]{:S(2)}) copy-start(bf16[512,256]{1,0:T(8,128)(2,1)} %param.19) | copy-start | bytes 786436
  4.2 13.5 %copy-start.3 = (bf16[512,256]{1,0:T(8,128)(2,1)S(1)}, bf16[512,256]{1,0:T(8,128)(2,1)}, u32[]{:S(2)}) copy-start(bf16[512,256]{1,0:T(8,128)(2,1)} %param.18) | copy-start | bytes 786436
  4.2 26.7 %copy-start.14 = (f32[128]{0:T(128)S(1)}, f32[128]{0:T(128)}, u32[]{:S(2)}) copy-start(f32[128]{0:T(128)} %param.21) | copy-start | bytes 1540
  5.3 50.7 %all-to-all-start = ((f16[8,64,512]{2,1,0:T(8,128)(2,1)}), f16[8,64,512]{2,1,0:T(8,128)(2,1)S(1)}, u32[]{:S(2)}, u32[]{:S(2)}) async-start(f16[8,64,512]{2,1,0:T(8,128)(2,1)} %fusion.1), calls=%async_computation | async-start | bytes 1048576 | tf_op jit(solution)/shard_map/all_to_all | solution.py:214
  10.3 9.7 %collective-permute-start = (f16[1,32,512]{2,1,0:T(8,128)(2,1)S(1)}, f16[1,32,512]{2,1,0:T(8,128)(2,1)S(1)}, u32[]{:S(2)}, u32[]{:S(2)}) collective-permute-start(f16[1,32,512]{2,1,0:T(8,128)(2,1)S(1)} %get-tuple-element.22), channel_id=1, source_target_pairs={{32,0},{40,8},{48,16},{56,24},{0,32},{8,40},{16,48},{24,56},{96,64... | collective-permute-start | bytes 98312 | tf_op jit(solution)/shard_map/weights/ppermute | solution.py:64
  20.0 13.6 %collective-permute-start.1 = (f16[2,32,512]{2,1,0:T(8,128)(2,1)S(1)}, f16[2,32,512]{2,1,0:T(8,128)(2,1)S(1)}, u32[]{:S(2)}, u32[]{:S(2)}) collective-permute-start(f16[2,32,512]{2,1,0:T(8,128)(2,1)S(1)} %pad_maximum_fusion.5), channel_id=1, source_target_pairs={{256,0},{264,8},{272,16},{280,24},{288,32},{296,40},{304,48},{312,... | collective-permute-start | bytes 196616 | tf_op jit(solution)/shard_map/weights/ppermute | solution.py:64
  33.7 12.2 %collective-permute-start.2 = (f16[4,32,512]{2,1,0:T(8,128)(2,1)S(1)}, f16[4,32,512]{2,1,0:T(8,128)(2,1)S(1)}, u32[]{:S(2)}, u32[]{:S(2)}) collective-permute-start(f16[4,32,512]{2,1,0:T(8,128)(2,1)S(1)} %pad_maximum_fusion.4), channel_id=1, source_target_pairs={{128,0},{136,8},{144,16},{152,24},{160,32},{168,40},{176,48},{184,... | collective-permute-start | bytes 393224 | tf_op jit(solution)/shard_map/weights/ppermute | solution.py:64
  46.6 20.9 %collective-permute-start.3 = (f16[8,32,512]{2,1,0:T(8,128)(2,1)}, f16[8,32,512]{2,1,0:T(8,128)(2,1)}, u32[]{:S(2)}, u32[]{:S(2)}) collective-permute-start(f16[8,32,512]{2,1,0:T(8,128)(2,1)} %pad_maximum_fusion), channel_id=1, source_target_pairs={{80,0},{88,8},{96,16},{104,24},{112,32},{120,40},{64,48},{72,56},{... | collective-permute-start | bytes 786440 | tf_op jit(solution)/shard_map/weights/ppermute | solution.py:64
  57.0 18.3 %copy-start.4 = (bf16[512,256]{1,0:T(8,128)(2,1)S(1)}, bf16[512,256]{1,0:T(8,128)(2,1)}, u32[]{:S(2)}) copy-start(bf16[512,256]{1,0:T(8,128)(2,1)} %param.17) | copy-start | bytes 786436
  57.0 18.1 %all-to-all-start.1 = ((f16[8,64,512]{2,1,0:T(8,128)(2,1)}), f16[8,64,512]{2,1,0:T(8,128)(2,1)S(1)}, u32[]{:S(2)}, u32[]{:S(2)}) async-start(f16[8,64,512]{2,1,0:T(8,128)(2,1)} %broadcast_in_dim.10), calls=%async_computation.1 | async-start | bytes 1048576 | tf_op jit(solution)/shard_map/all_to_all | solution.py:43
  62.6 13.0 %copy-start.8 = (bf16[512,128]{1,0:T(8,128)(2,1)S(1)}, bf16[512,128]{1,0:T(8,128)(2,1)}, u32[]{:S(2)}) copy-start(bf16[512,128]{1,0:T(8,128)(2,1)} %get-tuple-element.24) | copy-start | bytes 393220
  69.2 25.4 %collective-permute-start.5 = (f16[16,32,512]{2,1,0:T(8,128)(2,1)}, f16[16,32,512]{2,1,0:T(8,128)(2,1)}, u32[]{:S(2)}, u32[]{:S(2)}) collective-permute-start(f16[16,32,512]{2,1,0:T(8,128)(2,1)} %get-tuple-element.29), channel_id=1, source_target_pairs={{64,0},{72,8},{80,16},{88,24},{96,32},{104,40},{112,48},{120,56},{... | collective-permute-start | bytes 1572872 | tf_op jit(solution)/shard_map/weights/ppermute | solution.py:64
  71.1 22.3 %collective-permute-start.4 = (f16[16,32,512]{2,1,0:T(8,128)(2,1)}, f16[16,32,512]{2,1,0:T(8,128)(2,1)}, u32[]{:S(2)}, u32[]{:S(2)}) collective-permute-start(f16[16,32,512]{2,1,0:T(8,128)(2,1)} %get-tuple-element.29), channel_id=1, source_target_pairs={{8,0},{16,8},{24,16},{32,24},{40,32},{48,40},{56,48},{0,56},{72,64... | collective-permute-start | bytes 1572872 | tf_op jit(solution)/shard_map/weights/ppermute | solution.py:64
  75.9 11.6 %copy-start.1 = (s32[8,8]{1,0:T(8,128)S(1)}, s32[8,8]{1,0:T(8,128)}, u32[]{:S(2)}) copy-start(s32[8,8]{1,0:T(8,128)} %constant.80.clone) | copy-start | bytes 772
  77.5 23.3 %all-to-all-start.2 = ((f16[64,4,512]{2,1,0:T(4,128)(2,1)}), f16[64,4,512]{2,1,0:T(4,128)(2,1)S(1)}, u32[]{:S(2)}, u32[]{:S(2)}) async-start(f16[64,4,512]{2,1,0:T(4,128)(2,1)} %fusion.3), calls=%async_computation.2 | async-start | bytes 524288 | tf_op jit(solution)/shard_map/all_to_all | solution.py:225
  88.7 12.2 %copy-start.9 = (f32[4,256]{1,0:T(4,128)S(1)}, f32[4,256]{1,0:T(4,128)}, u32[]{:S(2)}) copy-start(f32[4,256]{1,0:T(4,128)} %param.30) | copy-start | bytes 12292
  88.7 12.2 %copy-start.10 = (f32[4,256]{1,0:T(4,128)S(1)}, f32[4,256]{1,0:T(4,128)}, u32[]{:S(2)}) copy-start(f32[4,256]{1,0:T(4,128)} %param.28) | copy-start | bytes 12292
  88.7 12.2 %copy-start.11 = (f32[4,256]{1,0:T(4,128)S(1)}, f32[4,256]{1,0:T(4,128)}, u32[]{:S(2)}) copy-start(f32[4,256]{1,0:T(4,128)} %param.29) | copy-start | bytes 12292
  88.7 12.3 %copy-start.12 = (f32[4,256]{1,0:T(4,128)S(1)}, f32[4,256]{1,0:T(4,128)}, u32[]{:S(2)}) copy-start(f32[4,256]{1,0:T(4,128)} %param.27) | copy-start | bytes 12292
  90.1 19.2 %collective-permute-start.6 = (f16[16,32,512]{2,1,0:T(8,128)(2,1)}, f16[16,32,512]{2,1,0:T(8,128)(2,1)S(1)}, u32[]{:S(2)}, u32[]{:S(2)}) collective-permute-start(f16[16,32,512]{2,1,0:T(8,128)(2,1)} %get-tuple-element.29), channel_id=1, source_target_pairs={{56,0},{0,8},{8,16},{16,24},{24,32},{32,40},{40,48},{48,56},{120,6... | collective-permute-start | bytes 1572872 | tf_op jit(solution)/shard_map/weights/ppermute | solution.py:64
  101.8 20.6 %all-to-all-start.3 = ((f16[64,4,512]{2,1,0:T(4,128)(2,1)}), f16[64,4,512]{2,1,0:T(4,128)(2,1)S(1)}, u32[]{:S(2)}, u32[]{:S(2)}) async-start(f16[64,4,512]{2,1,0:T(4,128)(2,1)} %broadcast_in_dim.11), calls=%async_computation.3 | async-start | bytes 524288 | tf_op jit(solution)/shard_map/all_to_all | solution.py:43

commit v3 on v1

v3 whole, which is shorter than its diff:
```python
import math

import jax
import jax.numpy as jnp
from jax import lax
from jax.experimental import pallas as pl
from jax.experimental.pallas import tpu as pltpu
from jax.sharding import PartitionSpec as P

F32 = jnp.float32
BF16 = jnp.bfloat16
F16 = jnp.float16

WEIGHT_LIMIT = 0.125
DIRECTION_LIMIT = 16.0
TOKEN_SCALE = 2.0**4
LOW_SCALE = 2.0**-2

CENTRE = 2.0**15.5
GROUP = 512
TOKEN_STEPS = 2


def coded(x, limit):
    size = jnp.maximum(jnp.abs(x) * (1.0 / limit), 2.0**-31) * CENTRE
    square = size * size
    fourth = square * square
    power = 1.0 / (fourth * fourth)
    return jnp.where(x < 0, -power, power).astype(BF16)


def decoded(code, limit):
    power = code.astype(F32)
    size = lax.rsqrt(lax.rsqrt(lax.rsqrt(jnp.abs(power)))) * (limit / CENTRE)
    return jnp.where(power < 0, -size, size)


def dot(left, right, left_dim, right_dim):
    return lax.dot_general(
        left, right, (((left_dim,), (right_dim,)), ((), ())), preferred_element_type=F32
    )


def two_parts(x):
    high = lax.reduce_precision(x, 8, 7)
    return high.astype(BF16), (x - high).astype(BF16)


def dot_two(left, right_parts, left_dim, right_dim):
    high, low = right_parts
    return dot(left, high, left_dim, right_dim) + dot(left, low, left_dim, right_dim)


def copy_for_each(x, axis):
    size = lax.axis_size(axis)
    return lax.all_to_all(jnp.broadcast_to(x[None], (size, *x.shape)), axis, 0, 0, tiled=True)


def normed_heads(first_map, second_map, lambdas, head_gain):
    width = head_gain.shape[0]
    heads = []
    for h in range(lambdas.shape[0]):
        cols = slice(h * width, (h + 1) * width)
        difference = first_map[:, cols].astype(F32) - lambdas[h] * second_map[:, cols].astype(F32)
        mean = jnp.mean(difference * difference, axis=-1, keepdims=True)
        heads.append((difference * lax.rsqrt(mean + 1e-06) * head_gain[None, :]).astype(BF16))
    return jnp.concatenate(heads, axis=1)


def project_kernel(place, inputs, cotangent, value_factor, output_factor, pieces):
    rank = value_factor.shape[1]
    rows = pieces.shape[:2]
    pieces[:, :, :rank] = dot(inputs[...], value_factor[...], 1, 0).astype(BF16).reshape(*rows, rank)
    pieces[:, :, rank:] = dot(cotangent[...], output_factor[...], 1, 0).astype(BF16).reshape(*rows, rank)


def project(place, inputs, cotangent, value_factor, output_factor, parts):
    tokens, cols = inputs.shape
    rank = value_factor.shape[1]
    return pl.pallas_call(
        project_kernel,
        grid_spec=pltpu.PrefetchScalarGridSpec(
            num_scalar_prefetch=1,
            grid=(TOKEN_STEPS,),
            in_specs=[
                pl.BlockSpec((tokens // TOKEN_STEPS, cols), lambda i, p: (i, 0)),
                pl.BlockSpec((tokens // TOKEN_STEPS, cols), lambda i, p: (i, 0)),
                pl.BlockSpec((cols, rank), lambda i, p: (p[0], 0)),
                pl.BlockSpec((cols, rank), lambda i, p: (p[0], 0)),
            ],
            out_specs=pl.BlockSpec(
                (parts // TOKEN_STEPS, tokens // parts, 2 * rank), lambda i, p: (i, 0, 0)
            ),
        ),
        out_shape=jax.ShapeDtypeStruct((parts, tokens // parts, 2 * rank), BF16),
        name="project",
    )(place, inputs, cotangent, value_factor, output_factor)


def last_kernel(
    weights,
    directions,
    value_factor,
    output_factor,
    own_value_factor,
    own_output_factor,
    value_weight,
    output_weight_t,
    value_copy,
    output_copy,
    value_master,
    output_master_t,
    high,
    low,
    high_t,
    low_t,
):
    cols = value_copy.shape[1]

    @pl.when(pl.program_id(0) == 0)
    def _():
        value = decoded(directions[:, :cols], 0.05 * DIRECTION_LIMIT)
        upper = value.astype(BF16)
        high[...] = upper
        low[...] = (value - upper.astype(F32)).astype(BF16)
        output = decoded(directions[:, cols:], 0.05 * DIRECTION_LIMIT).T
        upper = output.astype(BF16)
        high_t[...] = upper
        low_t[...] = (output - upper.astype(F32)).astype(BF16)
        value_master[...] = value_weight[...] - (
            dot(own_value_factor[...], high[...], 1, 0) + dot(own_value_factor[...], low[...], 1, 0)
        )
        output_master_t[...] = output_weight_t[...] - (
            dot(own_output_factor[...], high_t[...], 1, 1)
            + dot(own_output_factor[...], low_t[...], 1, 1)
        )

    old = decoded(weights[...], WEIGHT_LIMIT)
    value_step = dot(value_factor[...], high[...], 1, 0) + dot(value_factor[...], low[...], 1, 0)
    value_copy[...] = (old[:, :cols] - value_step).astype(BF16)
    output_step = dot(high_t[...], output_factor[...], 1, 1) + dot(
        low_t[...], output_factor[...], 1, 1
    )
    output_copy[...] = (old[:, cols:].T - output_step).astype(BF16)


def last_step(weights, directions, value_factor, output_factor, own_v, own_o, value_weight, output_weight_t):
    width, rank = value_factor.shape
    rows, cols = value_weight.shape
    whole = lambda *shape: pl.BlockSpec(shape, lambda i: (0,) * len(shape))
    return pl.pallas_call(
        last_kernel,
        grid=(width // GROUP,),
        in_specs=[
            pl.BlockSpec((GROUP, 2 * cols), lambda i: (i, 0)),
            whole(*directions.shape),
            pl.BlockSpec((GROUP, rank), lambda i: (i, 0)),
            pl.BlockSpec((GROUP, rank), lambda i: (i, 0)),
            whole(*own_v.shape),
            whole(*own_o.shape),
            whole(rows, cols),
            whole(rows, cols),
        ],
        out_specs=[
            pl.BlockSpec((GROUP, cols), lambda i: (i, 0)),
            pl.BlockSpec((cols, GROUP), lambda i: (0, i)),
            whole(rows, cols),
            whole(rows, cols),
        ],
        scratch_shapes=[
            pltpu.VMEM((rank, cols), BF16),
            pltpu.VMEM((rank, cols), BF16),
            pltpu.VMEM((cols, rank), BF16),
            pltpu.VMEM((cols, rank), BF16),
        ],
        out_shape=[
            jax.ShapeDtypeStruct((width, cols), BF16),
            jax.ShapeDtypeStruct((cols, width), BF16),
            jax.ShapeDtypeStruct((rows, cols), F32),
            jax.ShapeDtypeStruct((rows, cols), F32),
        ],
        name="last_step",
    )(weights, directions, value_factor, output_factor, own_v, own_o, value_weight, output_weight_t)


def local(
    inputs,
    value_cotangent,
    first_map,
    second_map,
    lambdas,
    head_gain,
    output_cotangent,
    value_factor,
    output_factor,
    value_weight,
    output_weight,
    value_moment,
    value_second,
    output_moment,
    output_second,
):
    tok_rows, cols = inputs.shape
    rank = value_factor.shape[1]
    fs_size, tp_size = lax.axis_size("fs"), lax.axis_size("tp")
    fs_index, tp_index = lax.axis_index("fs"), lax.axis_index("tp")
    width_rows = value_weight.shape[0]

    output_weight_t = output_weight.T
    own_weights = jnp.concatenate([value_weight, output_weight_t], axis=1)
    weights = lax.all_gather(coded(own_weights, WEIGHT_LIMIT), "fs", axis=0, tiled=True)

    place = jnp.full((1,), tp_index, jnp.int32)
    pieces = project(place, inputs, output_cotangent, value_factor, output_factor, tp_size)
    pieces = lax.all_to_all(pieces, "tp", 0, 0, tiled=True)
    summed = (jnp.sum(pieces.astype(F32), axis=0) * TOKEN_SCALE).astype(F16)
    tokens = copy_for_each(summed, "tp").reshape(tok_rows, 2 * rank).astype(F32)

    heads_out = normed_heads(first_map, second_map, lambdas, head_gain)
    scale = LOW_SCALE / (TOKEN_SCALE * math.sqrt(tok_rows * fs_size))
    token_parts = two_parts(tokens)
    low_value = dot_two(value_cotangent, [p[:, :rank] for p in token_parts], 0, 0)
    low_output = dot_two(heads_out, [p[:, rank:] for p in token_parts], 0, 0)
    partial = jnp.concatenate([low_value.T, low_output.T], axis=1) * scale
    tiles = partial.astype(F16).reshape(fs_size, -1, 2 * cols)
    tiles = lax.all_to_all(tiles, "fs", 0, 0, tiled=True)
    own_rows = jnp.sum(tiles.astype(F32), axis=0) * (1.0 / LOW_SCALE)

    moments = jnp.concatenate([value_moment, output_moment], axis=1)
    seconds = jnp.concatenate([value_second, output_second], axis=1)
    moment_new = 0.8 * moments + 0.2 * own_rows
    second_new = 0.95 * seconds + 0.05 * own_rows * own_rows
    direction = moment_new / (jnp.sqrt(second_new) + 1e-08)

    directions = copy_for_each(coded(direction, DIRECTION_LIMIT), "fs").reshape(rank, 2 * cols)
    own_v = lax.dynamic_slice_in_dim(value_factor, fs_index * width_rows, width_rows, 0)
    own_o = lax.dynamic_slice_in_dim(output_factor, fs_index * width_rows, width_rows, 0)
    value_copy, output_copy, value_master, output_master_t = last_step(
        weights, directions, value_factor, output_factor, own_v, own_o, value_weight, output_weight_t
    )
    return (
        value_master,
        output_master_t.T,
        moment_new[:, :cols],
        second_new[:, :cols],
        moment_new[:, cols:],
        second_new[:, cols:],
        value_copy,
        output_copy,
    )


def solution(mesh):
    rows_cols = P("fs", "tp")
    in_specs = (rows_cols,) * 4 + (P("tp"), P(), rows_cols, P(), P(), rows_cols, P("tp", "fs")) + (rows_cols,) * 4
    out_specs = (rows_cols, P("tp", "fs")) + (rows_cols,) * 4 + (P(None, "tp"), P("tp", None))
    return jax.shard_map(local, mesh=mesh, in_specs=in_specs, out_specs=out_specs, check_vma=False)
```

time: 145 us -> 116 us (0.80)
  the two profiles are of different devices: /device:TPU:8 before, /device:TPU:28 now
where the time goes in v3:
time: 116 us
  waiting for transfers between devices  46.4 us (40%)
  starting transfers between devices  34.3 us (30%)
  between operations  14.2 us (12%)
  Pallas kernels  8.3 us (7%)
  other arithmetic  5.8 us (5%)
  local copies, waits for them, and re-layouts  5.72 us (5%)
    all_to_all x2, waiting for transfers between devices, copy_for_each(): lax.all_to_all(jnp.broadcast_to(x[None], (size, *x.shape)), axis, 0, 0, t...  17 us
    all_to_all x1, starting transfers between devices, local(): tiles = lax.all_to_all(tiles, 'fs', 0, 0, tiled=True)  16.4 us
    all_to_all x1, waiting for transfers between devices, local(): tiles = lax.all_to_all(tiles, 'fs', 0, 0, tiled=True)  13.2 us
    all_to_all x2, starting transfers between devices, copy_for_each(): lax.all_to_all(jnp.broadcast_to(x[None], (size, *x.shape)), axis, 0, 0, t...  13 us
    all_gather x1, waiting for transfers between devices, local(): lax.all_gather(coded(own_weights, WEIGHT_LIMIT), 'fs', axis=0, tiled=True)  11.2 us
    pallas_call x1, Pallas kernels, last_step(): pl.pallas_call(last_kernel, grid=(width // GROUP,), in_specs=[pl.BlockSpe...  5.93 us
    all_to_all x1, waiting for transfers between devices, local(): pieces = lax.all_to_all(pieces, 'tp', 0, 0, tiled=True)  5.08 us
    all_to_all x1, starting transfers between devices, local(): pieces = lax.all_to_all(pieces, 'tp', 0, 0, tiled=True)  4.93 us
  transfers between devices with their start and end apart: 5, of which 5 were waited for; matrix products, arithmetic and copies ran while one was open for 10% of the time, Pallas kernels for 2%

profile of v3, /device:TPU:28, one launch (start us, length us, event | category | flops | bytes accessed | tf_op | source)
XLA Modules:
  0.0 115.9 jit_solution(13378702717051941629)
XLA Ops:
  7.2 0.0 all-gather.2.cloned.1.call-start
  7.2 1.5 %fusion.8 = bf16[32,512]{1,0:T(8,128)(2,1)} fusion(f32[32,256]{1,0:T(8,128)} %bitcast.11, f32[32,256]{1,0:T(8,128)} %value_weight.1), kind=kLoop, calls=%fused_computation.24 | loop fusion | flops 212992 | bytes 98304 | tf_op jit(solution)/shard_map/convert_element_type | solution.py:29
  8.8 2.4 %project.1 = bf16[8,64,512]{2,1,0:T(8,128)(2,1)} custom-call(s32[1]{0:T(128)} %bitcast.1.place, bf16[512,256]{1,0:T(8,128)(2,1)} %inputs.1, bf16[512,256]{1,0:T(8,128)(2,1)} %cotangent.1, bf16[2048,256]{1,0:T(8,128)(2,1)} %value_factor.3, bf16[2048,256]{1,0:T(8,128)(2,1)} %output_factor.3), custom_call_target="tpu_custom_call" | custom-call | tf_op jit(solution)/shard_map/project/pallas_call | solution.py:80
  11.1 4.9 %all-to-all-start = ((bf16[8,64,512]{2,1,0:T(8,128)(2,1)}), bf16[8,64,512]{2,1,0:T(8,128)(2,1)S(1)}, u32[]{:S(2)}, u32[]{:S(2)}) async-start(bf16[8,64,512]{2,1,0:T(8,128)(2,1)} %project.1), calls=%async_computation | async-start | bytes 1048576 | tf_op jit(solution)/shard_map/all_to_all | solution.py:215
  16.1 0.6 fusion.18
  16.6 1.5 %multiply_reduce_fusion.1 = (f32[512]{0:T(512)S(1)}, f32[512]{0:T(512)S(1)}) fusion(f32[]{:T(128)} %bitcast.4, bf16[512,256]{1,0:T(8,128)(2,1)S(1)} %copy-done.1, bf16[512,256]{1,0:T(8,128)(2,1)S(1)} %copy-done.2, f32[]{:T(128)} %bitcast.5), kind=kLoop, calls=%fused_computation.20 | loop fusion | flops 785408 | bytes 528392 | tf_op jit(solution)/shard_map/reduce_sum | solution.py:65
  18.2 5.1 %all-to-all-done = bf16[8,64,512]{2,1,0:T(8,128)(2,1)S(1)} async-done(((bf16[8,64,512]{2,1,0:T(8,128)(2,1)}), bf16[8,64,512]{2,1,0:T(8,128)(2,1)S(1)}, u32[]{:S(2)}, u32[]{:S(2)}) %all-to-all-start) | async-done | bytes 524320 | tf_op jit(solution)/shard_map/all_to_all | solution.py:215
  23.2 0.1 convert_reduce_fusion
  23.3 0.8 broadcast_in_dim.7
  24.2 6.6 %all-to-all-start.1 = ((f16[8,64,512]{2,1,0:T(8,128)(2,1)}), f16[8,64,512]{2,1,0:T(8,128)(2,1)S(1)}, u32[]{:S(2)}, u32[]{:S(2)}) async-start(f16[8,64,512]{2,1,0:T(8,128)(2,1)} %broadcast_in_dim.7), calls=%async_computation.1 | async-start | bytes 1048576 | tf_op jit(solution)/shard_map/all_to_all | solution.py:56
  30.7 1.5 %multiply_convert_fusion.1 = (bf16[512,128]{1,0:T(8,128)(2,1)S(1)}, bf16[512,128]{1,0:T(8,128)(2,1)S(1)}) fusion(f32[128]{0:T(128)S(1)} %copy-done.8, f32[512]{0:T(512)S(1)} %get-tuple-element.32, f32[]{:T(128)} %bitcast.4, bf16[512,256]{1,0:T(8,128)(2,1)S(1)} %copy-done.1, bf16[512,256]{1,0:T(8,128)(2,1)S(1)} %copy-done.2, f32[512]{0:T(512)S(1)} %get-tuple-element.31, ...), kind=kLoop, calls=%fused_computation.19 | loop fusion | flops 917504 | bytes 791048 | tf_op jit(solution)/shard_map/convert_element_type | solution.py:66
  32.3 5.6 %all-to-all-done.1 = f16[8,64,512]{2,1,0:T(8,128)(2,1)S(1)} async-done(((f16[8,64,512]{2,1,0:T(8,128)(2,1)}), f16[8,64,512]{2,1,0:T(8,128)(2,1)S(1)}, u32[]{:S(2)}, u32[]{:S(2)}) %all-to-all-start.1) | async-done | bytes 524320 | tf_op jit(solution)/shard_map/all_to_all | solution.py:56
  37.9 0.2 fusion
  38.1 0.3 fusion.6
  38.4 0.3 convolution_add_fusion.1
  38.6 0.1 concatenate.30
  38.8 0.3 fusion.3
  39.0 0.3 convolution_add_fusion
  39.3 0.1 concatenate.32
  39.4 0.9 fusion.1
  40.3 16.4 %all-to-all-start.2 = ((f16[64,4,512]{2,1,0:T(4,128)(2,1)}), f16[64,4,512]{2,1,0:T(4,128)(2,1)S(1)}, u32[]{:S(2)}, u32[]{:S(2)}) async-start(f16[64,4,512]{2,1,0:T(4,128)(2,1)} %fusion.1), calls=%async_computation.2 | async-start | bytes 524288 | tf_op jit(solution)/shard_map/all_to_all | solution.py:226
  56.6 13.2 %all-to-all-done.2 = f16[64,4,512]{2,1,0:T(4,128)(2,1)S(1)} async-done(((f16[64,4,512]{2,1,0:T(4,128)(2,1)}), f16[64,4,512]{2,1,0:T(4,128)(2,1)S(1)}, u32[]{:S(2)}, u32[]{:S(2)}) %all-to-all-start.2) | async-done | bytes 262176 | tf_op jit(solution)/shard_map/all_to_all | solution.py:226
  69.8 0.1 convert_reduce_fusion.1
  70.0 0.8 broadcast_in_dim.8
  70.8 6.4 %all-to-all-start.3 = ((bf16[64,4,512]{2,1,0:T(4,128)(2,1)}), bf16[64,4,512]{2,1,0:T(4,128)(2,1)S(1)}, u32[]{:S(2)}, u32[]{:S(2)}) async-start(bf16[64,4,512]{2,1,0:T(4,128)(2,1)} %broadcast_in_dim.8), calls=%async_computation.3 | async-start | bytes 524288 | tf_op jit(solution)/shard_map/all_to_all | solution.py:56
  77.2 1.4 %constant_dynamic-slice_fusion = (bf16[32,256]{1,0:T(8,128)(2,1)}, bf16[32,256]{1,0:T(8,128)(2,1)}) fusion(bf16[2048,256]{1,0:T(8,128)(2,1)} %output_factor.3, s32[]{:T(128)S(6)} %select_n.18, bf16[2048,256]{1,0:T(8,128)(2,1)} %value_factor.3), kind=kLoop, calls=%fused_computation.35 | loop fusion | bytes 65540 | tf_op jit(solution)/shard_map/dynamic_slice | solution.py:237
  78.6 0.6 fusion.16
  79.2 0.6 fusion.17
  79.8 11.4 %all-to-all-done.3 = bf16[64,4,512]{2,1,0:T(4,128)(2,1)S(1)} async-done(((bf16[64,4,512]{2,1,0:T(4,128)(2,1)}), bf16[64,4,512]{2,1,0:T(4,128)(2,1)S(1)}, u32[]{:S(2)}, u32[]{:S(2)}) %all-to-all-start.3) | async-done | bytes 262176 | tf_op jit(solution)/shard_map/all_to_all | solution.py:56
  91.1 0.8 reshape.99.directions
  91.9 11.2 %all-gather.2.cloned.1.call-done.weights = bf16[2048,512]{1,0:T(8,128)(2,1)} async-done(((bf16[32,512]{1,0:T(8,128)(2,1)}), bf16[2048,512]{1,0:T(8,128)(2,1)}) %all-gather.2.cloned.1.call-update) | async-done | bytes 2097168 | tf_op jit(solution)/shard_map/all_gather | solution.py:211
  103.1 5.9 %last_step.1 = (bf16[2048,256]{1,0:T(8,128)(2,1)}, bf16[256,2048]{1,0:T(8,128)(2,1)}, f32[32,256]{1,0:T(8,128)}, f32[32,256]{1,0:T(8,128)}) custom-call(bf16[2048,512]{1,0:T(8,128)(2,1)} %all-gather.2.cloned.1.call-done.weights, bf16[256,512]{1,0:T(8,128)(2,1)} %reshape.99.directions, bf16[2048,256]{1,0:T(8,128)(2,1)} %value_factor.3, ...), custom_call_target="tpu_custom_call" | custom-call | tf_op jit(solution)/shard_map/last_step/pallas_call | solution.py:151
  (22 shorter events, 0.1 us)
Async XLA Ops:
  7.2 30.9 %copy-start = (bf16[512,256]{1,0:T(8,128)(2,1)S(1)}, bf16[512,256]{1,0:T(8,128)(2,1)}, u32[]{:S(2)}) copy-start(bf16[512,256]{1,0:T(8,128)(2,1)} %param.16) | copy-start | bytes 786436
  7.2 95.9 %all-gather.2.cloned.1.call-start = ((), (), s32[]{:S(2)}) async-start(), calls=%async_computation.4 | async-start | bytes 2129920 | tf_op jit(solution)/shard_map/all_gather | solution.py:211
  8.7 7.3 %copy-start.7 = (f32[2]{0:T(128)S(1)}, f32[2]{0:T(128)}, u32[]{:S(2)}) copy-start(f32[2]{0:T(128)} %param.19) | copy-start | bytes 28
  8.7 7.9 %copy-start.1 = (bf16[512,256]{1,0:T(8,128)(2,1)S(1)}, bf16[512,256]{1,0:T(8,128)(2,1)}, u32[]{:S(2)}) copy-start(bf16[512,256]{1,0:T(8,128)(2,1)} %param.18) | copy-start | bytes 786436
  8.7 7.9 %copy-start.2 = (bf16[512,256]{1,0:T(8,128)(2,1)S(1)}, bf16[512,256]{1,0:T(8,128)(2,1)}, u32[]{:S(2)}) copy-start(bf16[512,256]{1,0:T(8,128)(2,1)} %param.17) | copy-start | bytes 786436
  11.1 19.6 %copy-start.8 = (f32[128]{0:T(128)S(1)}, f32[128]{0:T(128)}, u32[]{:S(2)}) copy-start(f32[128]{0:T(128)} %param.20) | copy-start | bytes 1540
  11.1 12.1 %all-to-all-start = ((bf16[8,64,512]{2,1,0:T(8,128)(2,1)}), bf16[8,64,512]{2,1,0:T(8,128)(2,1)S(1)}, u32[]{:S(2)}, u32[]{:S(2)}) async-start(bf16[8,64,512]{2,1,0:T(8,128)(2,1)} %project.1), calls=%async_computation | async-start | bytes 1048576 | tf_op jit(solution)/shard_map/all_to_all | solution.py:215
  24.2 13.7 %all-to-all-start.1 = ((f16[8,64,512]{2,1,0:T(8,128)(2,1)}), f16[8,64,512]{2,1,0:T(8,128)(2,1)S(1)}, u32[]{:S(2)}, u32[]{:S(2)}) async-start(f16[8,64,512]{2,1,0:T(8,128)(2,1)} %broadcast_in_dim.7), calls=%async_computation.1 | async-start | bytes 1048576 | tf_op jit(solution)/shard_map/all_to_all | solution.py:56
  38.7 31.2 %copy-start.3 = (f32[4,256]{1,0:T(4,128)S(1)}, f32[4,256]{1,0:T(4,128)}, u32[]{:S(2)}) copy-start(f32[4,256]{1,0:T(4,128)} %param.29) | copy-start | bytes 12292
  38.7 31.2 %copy-start.4 = (f32[4,256]{1,0:T(4,128)S(1)}, f32[4,256]{1,0:T(4,128)}, u32[]{:S(2)}) copy-start(f32[4,256]{1,0:T(4,128)} %param.27) | copy-start | bytes 12292
  38.7 31.2 %copy-start.5 = (f32[4,256]{1,0:T(4,128)S(1)}, f32[4,256]{1,0:T(4,128)}, u32[]{:S(2)}) copy-start(f32[4,256]{1,0:T(4,128)} %param.28) | copy-start | bytes 12292
  38.8 31.2 %copy-start.6 = (f32[4,256]{1,0:T(4,128)S(1)}, f32[4,256]{1,0:T(4,128)}, u32[]{:S(2)}) copy-start(f32[4,256]{1,0:T(4,128)} %param.26) | copy-start | bytes 12292
  40.3 29.5 %all-to-all-start.2 = ((f16[64,4,512]{2,1,0:T(4,128)(2,1)}), f16[64,4,512]{2,1,0:T(4,128)(2,1)S(1)}, u32[]{:S(2)}, u32[]{:S(2)}) async-start(f16[64,4,512]{2,1,0:T(4,128)(2,1)} %fusion.1), calls=%async_computation.2 | async-start | bytes 524288 | tf_op jit(solution)/shard_map/all_to_all | solution.py:226
  70.8 20.3 %all-to-all-start.3 = ((bf16[64,4,512]{2,1,0:T(4,128)(2,1)}), bf16[64,4,512]{2,1,0:T(4,128)(2,1)S(1)}, u32[]{:S(2)}, u32[]{:S(2)}) async-start(bf16[64,4,512]{2,1,0:T(4,128)(2,1)} %broadcast_in_dim.8), calls=%async_computation.3 | async-start | bytes 524288 | tf_op jit(solution)/shard_map/all_to_all | solution.py:56
Sparse Core Ops, SparseCore 0:
  11.6 91.4 all-gather.1

commit v4 on v3

--- a/solution.py
+++ b/solution.py
@@ -5,11 +5,14 @@
 from jax import lax
 from jax.experimental import pallas as pl
 from jax.experimental.pallas import tpu as pltpu
-from jax.sharding import PartitionSpec as P
+from jax.sharding import Mesh, PartitionSpec as P
 
 F32 = jnp.float32
 BF16 = jnp.bfloat16
 F16 = jnp.float16
+
+FS = ("z_far", "z_high", "z_low", "y_high", "y_low")
+Z, Y = FS[:3], FS[3:]
 
 WEIGHT_LIMIT = 0.125
 DIRECTION_LIMIT = 16.0
@@ -19,6 +22,7 @@
 CENTRE = 2.0**15.5
 GROUP = 512
 TOKEN_STEPS = 2
+NEAR_Y = 4
 
 
 def coded(x, limit):
@@ -65,6 +69,19 @@
         mean = jnp.mean(difference * difference, axis=-1, keepdims=True)
         heads.append((difference * lax.rsqrt(mean + 1e-06) * head_gain[None, :]).astype(BF16))
     return jnp.concatenate(heads, axis=1)
+
+
+def from_offset(x, dy, dz):
+    nz, ny = lax.axis_size(Z), lax.axis_size(Y)
+    pairs = []
+    for z in range(nz):
+        for y in range(ny):
+            pairs.append((((z + dz) % nz) * ny + (y + dy) % ny, z * ny + y))
+    return lax.ppermute(x, FS, pairs)
+
+
+def all_quarters(own):
+    return own, from_offset(own, 1, 0), from_offset(own, 0, -1), from_offset(own, -1, 1)
 
 
 def project_kernel(place, inputs, cotangent, value_factor, output_factor, pieces):
@@ -97,6 +114,38 @@
     )(place, inputs, cotangent, value_factor, output_factor)
 
 
+def arrange_kernel(place, own, other_y, other_z, others, weights):
+    rows = own.shape[2]
+    z_size, y_size = place[2], place[3]
+    steps = ((own, 0, 0), (other_y, 0, 1), (other_z, -1, 0), (others, 1, 1))
+    for quarter, z_step, y_step in steps:
+        holder = (place[0] + z_size + z_step) % z_size
+        y_low = (place[1] + y_step) % 2
+        for near in range(quarter.shape[0]):
+            for slot in range(2):
+                z_far = (holder // (z_size // 2) + slot) % 2
+                z = z_far * (z_size // 2) + near // NEAR_Y * 2 + holder % 2
+                y = near % NEAR_Y * 2 + y_low
+                at = pl.multiple_of((z * y_size + y) * rows, rows)
+                weights[pl.ds(at, rows), :] = decoded(quarter[near, slot], WEIGHT_LIMIT)
+
+
+def arrange(place, quarters, width):
+    cols = quarters[0].shape[-1]
+    return pl.pallas_call(
+        arrange_kernel,
+        grid_spec=pltpu.PrefetchScalarGridSpec(
+            num_scalar_prefetch=1,
+            grid=(1,),
+            in_specs=[pl.BlockSpec(q.shape, lambda i, p: (0,) * 4) for q in quarters],
+            out_specs=pl.BlockSpec((width, cols), lambda i, p: (0, 0)),
+        ),
+        out_shape=jax.ShapeDtypeStruct((width, cols), F32),
+        cost_estimate=pl.CostEstimate(flops=60 * width * cols, bytes_accessed=6 * width * cols, transcendentals=0),
+        name="arrange",
+    )(place, *quarters)
+
+
 def last_kernel(
     weights,
     directions,
@@ -119,11 +168,12 @@
 
     @pl.when(pl.program_id(0) == 0)
     def _():
-        value = decoded(directions[:, :cols], 0.05 * DIRECTION_LIMIT)
+        whole = decoded(directions[...], 0.05 * DIRECTION_LIMIT).reshape(high.shape[0], -1)
+        value = whole[:, :cols]
         upper = value.astype(BF16)
         high[...] = upper
         low[...] = (value - upper.astype(F32)).astype(BF16)
-        output = decoded(directions[:, cols:], 0.05 * DIRECTION_LIMIT).T
+        output = whole[:, cols:].T
         upper = output.astype(BF16)
         high_t[...] = upper
         low_t[...] = (output - upper.astype(F32)).astype(BF16)
@@ -135,13 +185,12 @@
             + dot(own_output_factor[...], low_t[...], 1, 1)
         )
 
-    old = decoded(weights[...], WEIGHT_LIMIT)
     value_step = dot(value_factor[...], high[...], 1, 0) + dot(value_factor[...], low[...], 1, 0)
-    value_copy[...] = (old[:, :cols] - value_step).astype(BF16)
+    value_copy[...] = (weights[:, :cols] - value_step).astype(BF16)
     output_step = dot(high_t[...], output_factor[...], 1, 1) + dot(
         low_t[...], output_factor[...], 1, 1
     )
-    output_copy[...] = (old[:, cols:].T - output_step).astype(BF16)
+    output_copy[...] = (weights[:, cols:].T - output_step).astype(BF16)
 
 
 def last_step(weights, directions, value_factor, output_factor, own_v, own_o, value_weight, output_weight_t):
@@ -183,7 +232,7 @@
     )(weights, directions, value_factor, output_factor, own_v, own_o, value_weight, output_weight_t)
 
 
-def local(
+def update(
     inputs,
     value_cotangent,
     first_map,
@@ -202,19 +251,22 @@
 ):
     tok_rows, cols = inputs.shape
     rank = value_factor.shape[1]
-    fs_size, tp_size = lax.axis_size("fs"), lax.axis_size("tp")
-    fs_index, tp_index = lax.axis_index("fs"), lax.axis_index("tp")
+    fs_size, tp_size = lax.axis_size(FS), lax.axis_size("tp")
+    fs_index, tp_index = lax.axis_index(FS), lax.axis_index("tp")
     width_rows = value_weight.shape[0]
 
     output_weight_t = output_weight.T
     own_weights = jnp.concatenate([value_weight, output_weight_t], axis=1)
-    weights = lax.all_gather(coded(own_weights, WEIGHT_LIMIT), "fs", axis=0, tiled=True)
+    code = coded(own_weights, WEIGHT_LIMIT)
 
     place = jnp.full((1,), tp_index, jnp.int32)
     pieces = project(place, inputs, output_cotangent, value_factor, output_factor, tp_size)
+    far = from_offset(code, 0, lax.axis_size(Z) // 2)
     pieces = lax.all_to_all(pieces, "tp", 0, 0, tiled=True)
     summed = (jnp.sum(pieces.astype(F32), axis=0) * TOKEN_SCALE).astype(F16)
-    tokens = copy_for_each(summed, "tp").reshape(tok_rows, 2 * rank).astype(F32)
+    summed, far = lax.optimization_barrier((summed, far))
+    own_quarter = copy_for_each(jnp.stack([code, far]), ("z_high", "y_high")).reshape(-1, 2, *code.shape)
+    tokens = lax.all_gather(summed, "tp", axis=0, tiled=True).astype(F32)
 
     heads_out = normed_heads(first_map, second_map, lambdas, head_gain)
     scale = LOW_SCALE / (TOKEN_SCALE * math.sqrt(tok_rows * fs_size))
@@ -222,8 +274,10 @@
     low_value = dot_two(value_cotangent, [p[:, :rank] for p in token_parts], 0, 0)
     low_output = dot_two(heads_out, [p[:, rank:] for p in token_parts], 0, 0)
     partial = jnp.concatenate([low_value.T, low_output.T], axis=1) * scale
+    partial, own_quarter = lax.optimization_barrier((partial, own_quarter))
+    weights = all_quarters(own_quarter)
     tiles = partial.astype(F16).reshape(fs_size, -1, 2 * cols)
-    tiles = lax.all_to_all(tiles, "fs", 0, 0, tiled=True)
+    tiles = lax.all_to_all(tiles, FS, 0, 0, tiled=True)
     own_rows = jnp.sum(tiles.astype(F32), axis=0) * (1.0 / LOW_SCALE)
 
     moments = jnp.concatenate([value_moment, output_moment], axis=1)
@@ -232,11 +286,14 @@
     second_new = 0.95 * seconds + 0.05 * own_rows * own_rows
     direction = moment_new / (jnp.sqrt(second_new) + 1e-08)
 
-    directions = copy_for_each(coded(direction, DIRECTION_LIMIT), "fs").reshape(rank, 2 * cols)
+    directions = copy_for_each(coded(direction, DIRECTION_LIMIT), FS)
     own_v = lax.dynamic_slice_in_dim(value_factor, fs_index * width_rows, width_rows, 0)
     own_o = lax.dynamic_slice_in_dim(output_factor, fs_index * width_rows, width_rows, 0)
+    parities = [lax.axis_index(Z), lax.axis_index(Y), lax.axis_size(Z), lax.axis_size(Y)]
+    at = jnp.stack([jnp.int32(p) for p in parities])
+    old = arrange(at, weights, value_factor.shape[0])
     value_copy, output_copy, value_master, output_master_t = last_step(
-        weights, directions, value_factor, output_factor, own_v, own_o, value_weight, output_weight_t
+        old, directions, value_factor, output_factor, own_v, own_o, value_weight, output_weight_t
     )
     return (
         value_master,
@@ -251,7 +308,9 @@
 
 
 def solution(mesh):
-    rows_cols = P("fs", "tp")
-    in_specs = (rows_cols,) * 4 + (P("tp"), P(), rows_cols, P(), P(), rows_cols, P("tp", "fs")) + (rows_cols,) * 4
-    out_specs = (rows_cols, P("tp", "fs")) + (rows_cols,) * 4 + (P(None, "tp"), P("tp", None))
-    return jax.shard_map(local, mesh=mesh, in_specs=in_specs, out_specs=out_specs, check_vma=False)
+    fs, tp = mesh.devices.shape
+    fine = Mesh(mesh.devices.reshape(2, 2, 2, fs // 16, 2, tp), (*FS, "tp"))
+    rows_cols = P(FS, "tp")
+    in_specs = (rows_cols,) * 4 + (P("tp"), P(), rows_cols, P(), P(), rows_cols, P("tp", FS)) + (rows_cols,) * 4
+    out_specs = (rows_cols, P("tp", FS)) + (rows_cols,) * 4 + (P(None, "tp"), P("tp", None))
+    return jax.shard_map(update, mesh=fine, in_specs=in_specs, out_specs=out_specs, check_vma=False)

time: 116 us -> 112 us (0.966)
  the two profiles are of different devices: /device:TPU:28 before, /device:TPU:8 now
where the time goes in v4:
time: 112 us
  starting transfers between devices  51.5 us (46%)
  waiting for transfers between devices  17.5 us (16%)
  Pallas kernels  14.2 us (13%)
  blocking collectives  13.1 us (12%)
  local copies, waits for them, and re-layouts  8.37 us (7%)
  other arithmetic  5.04 us (4%)
    ppermute x4, starting transfers between devices, from_offset(): return lax.ppermute(x, FS, pairs)  21.1 us
    all_to_all x2, starting transfers between devices, copy_for_each(): lax.all_to_all(jnp.broadcast_to(x[None], (size, *x.shape)), axis, 0, 0, t...  17.5 us
    all_gather x1, blocking collectives, update(): tokens = lax.all_gather(summed, 'tp', axis=0, tiled=True).astype(F32)  13.1 us
    all_to_all x1, starting transfers between devices, update(): tiles = lax.all_to_all(tiles, FS, 0, 0, tiled=True)  8.61 us
    all_to_all x2, waiting for transfers between devices, copy_for_each(): lax.all_to_all(jnp.broadcast_to(x[None], (size, *x.shape)), axis, 0, 0, t...  7.32 us
    all_to_all x1, waiting for transfers between devices, update(): pieces = lax.all_to_all(pieces, 'tp', 0, 0, tiled=True)  6.61 us
    pallas_call x1, Pallas kernels, last_step(): pl.pallas_call(last_kernel, grid=(width // GROUP,), in_specs=[pl.BlockSpe...  6.07 us
    pallas_call x1, Pallas kernels, arrange(): pl.pallas_call(arrange_kernel, grid_spec=pltpu.PrefetchScalarGridSpec(num...  5.76 us
  transfers between devices with their start and end apart: 8, of which 4 were waited for; matrix products, arithmetic and copies ran while one was open for 8% of the time, Pallas kernels for 7%

profile of v4, /device:TPU:8, one launch (start us, length us, event | category | flops | bytes accessed | tf_op | source)
XLA Modules:
  0.0 111.6 jit_solution(12302765893522899419)
XLA Ops:
  0.7 0.9 fusion.7
  1.6 10.9 %collective-permute-start = (bf16[32,512]{1,0:T(8,128)(2,1)S(1)}, bf16[32,512]{1,0:T(8,128)(2,1)S(1)}, u32[]{:S(2)}, u32[]{:S(2)}) collective-permute-start(bf16[32,512]{1,0:T(8,128)(2,1)S(1)} %fusion.7), channel_id=1, source_target_pairs={{256,0},{264,8},{272,16},{280,24},{288,32},{296,40},{304,48},{312,... | collective-permute-start | bytes 98312 | tf_op jit(solution)/shard_map/ppermute | solution.py:80
  12.5 2.3 %project.1 = bf16[8,64,512]{2,1,0:T(8,128)(2,1)} custom-call(s32[1]{0:T(128)} %bitcast.2.place, bf16[512,256]{1,0:T(8,128)(2,1)} %inputs.1, bf16[512,256]{1,0:T(8,128)(2,1)} %cotangent.1, bf16[2048,256]{1,0:T(8,128)(2,1)} %value_factor.3, bf16[2048,256]{1,0:T(8,128)(2,1)} %output_factor.3), custom_call_target="tpu_custom_call" | custom-call | tf_op jit(solution)/shard_map/project/pallas_call | solution.py:97
  14.8 4.3 %all-to-all-start = ((bf16[8,64,512]{2,1,0:T(8,128)(2,1)}), bf16[8,64,512]{2,1,0:T(8,128)(2,1)S(1)}, u32[]{:S(2)}, u32[]{:S(2)}) async-start(bf16[8,64,512]{2,1,0:T(8,128)(2,1)} %project.1), calls=%async_computation | async-start | bytes 1048576 | tf_op jit(solution)/shard_map/all_to_all | solution.py:265
  19.1 0.6 fusion.18
  19.8 1.5 %multiply_reduce_fusion.1 = (f32[512]{0:T(512)S(1)}, f32[512]{0:T(512)S(1)}) fusion(f32[]{:T(128)} %bitcast.4, bf16[512,256]{1,0:T(8,128)(2,1)S(1)} %copy-done.3, bf16[512,256]{1,0:T(8,128)(2,1)S(1)} %copy-done.4, f32[]{:T(128)} %bitcast.5), kind=kLoop, calls=%fused_computation.19 | loop fusion | flops 785408 | bytes 528392 | tf_op jit(solution)/shard_map/reduce_sum | solution.py:69
  21.3 1.5 %multiply_convert_fusion.1 = (bf16[512,128]{1,0:T(8,128)(2,1)S(1)}, bf16[512,128]{1,0:T(8,128)(2,1)S(1)}) fusion(f32[128]{0:T(128)S(1)} %copy-done.15, f32[512]{0:T(512)S(1)} %get-tuple-element.40, f32[]{:T(128)} %bitcast.4, bf16[512,256]{1,0:T(8,128)(2,1)S(1)} %copy-done.3, bf16[512,256]{1,0:T(8,128)(2,1)S(1)} %copy-done.4, f32[512]{0:T(512)S(1)} %get-tuple-element.39, ...), kind=kLoop, calls=%fused_computation.18 | loop fusion | flops 917504 | bytes 791048 | tf_op jit(solution)/shard_map/convert_element_type | solution.py:70
  22.8 6.6 %all-to-all-done = bf16[8,64,512]{2,1,0:T(8,128)(2,1)S(1)} async-done(((bf16[8,64,512]{2,1,0:T(8,128)(2,1)}), bf16[8,64,512]{2,1,0:T(8,128)(2,1)S(1)}, u32[]{:S(2)}, u32[]{:S(2)}) %all-to-all-start) | async-done | bytes 524320 | tf_op jit(solution)/shard_map/all_to_all | solution.py:265
  29.6 0.8 broadcast_in_dim.7
  30.4 8.0 %all-to-all-start.1 = ((bf16[8,2,32,512]{3,2,1,0:T(8,128)(2,1)}), bf16[8,2,32,512]{3,2,1,0:T(8,128)(2,1)S(1)}, u32[]{:S(2)}, u32[]{:S(2)}) async-start(bf16[8,2,32,512]{3,2,1,0:T(8,128)(2,1)} %broadcast_in_dim.7), calls=%async_computation.1 | async-start | bytes 1048576 | tf_op jit(solution)/shard_map/all_to_all | solution.py:60
  38.4 13.1 %all_gather.3 = f16[512,512]{1,0:T(8,128)(2,1)S(1)} all-gather(f16[64,512]{1,0:T(8,128)(2,1)S(1)} %multiply_convert_fusion.2), channel_id=1, replica_groups=mesh['z_far'=2,'z_high'=2,'z_low'=2,'y_high'=4,'y_low'=2,'tp'=8] {'tp'}, dimensions={0}, use_global_device_ids=true | all-gather | bytes 589824 | tf_op jit(solution)/shard_map/all_gather | solution.py:269
  51.7 0.3 fusion.2
  52.0 0.3 fusion.5
  52.9 3.2 %all-to-all-done.1.own = bf16[8,2,32,512]{3,2,1,0:T(8,128)(2,1)S(1)} async-done(((bf16[8,2,32,512]{3,2,1,0:T(8,128)(2,1)}), bf16[8,2,32,512]{3,2,1,0:T(8,128)(2,1)S(1)}, u32[]{:S(2)}, u32[]{:S(2)}) %all-to-all-start.1) | async-done | bytes 524320 | tf_op jit(solution)/shard_map/all_to_all | solution.py:60
  56.5 0.8 reshape.176
  57.2 8.6 %all-to-all-start.2 = ((f16[64,4,512]{2,1,0:T(4,128)(2,1)}), f16[64,4,512]{2,1,0:T(4,128)(2,1)S(1)}, u32[]{:S(2)}, u32[]{:S(2)}) async-start(f16[64,4,512]{2,1,0:T(4,128)(2,1)} %reshape.176), calls=%async_computation.2 | async-start | bytes 524288 | tf_op jit(solution)/shard_map/all_to_all | solution.py:280
  65.9 1.4 %constant_dynamic-slice_fusion = (bf16[32,256]{1,0:T(8,128)(2,1)}, bf16[32,256]{1,0:T(8,128)(2,1)}) fusion(bf16[2048,256]{1,0:T(8,128)(2,1)} %output_factor.3, s32[]{:T(128)S(6)} %select_n.28, bf16[2048,256]{1,0:T(8,128)(2,1)} %value_factor.3), kind=kLoop, calls=%fused_computation.39 | loop fusion | bytes 65540 | tf_op jit(solution)/shard_map/dynamic_slice | solution.py:291
  67.2 5.7 %collective-permute-start.3 = (bf16[8,2,32,512]{3,2,1,0:T(8,128)(2,1)S(1)}, bf16[8,2,32,512]{3,2,1,0:T(8,128)(2,1)S(1)}, u32[]{:S(2)}, u32[]{:S(2)}) collective-permute-start(bf16[8,2,32,512]{3,2,1,0:T(8,128)(2,1)S(1)} %all-to-all-done.1.own), channel_id=1, source_target_pairs={{120,0},{64,8},{72,16},{80,24},{88,32},{96,40},{104,48},{112,56},{... | collective-permute-start | bytes 1572872 | tf_op jit(solution)/shard_map/ppermute | solution.py:80
  73.0 1.9 %collective-permute-start.2 = (bf16[8,2,32,512]{3,2,1,0:T(8,128)(2,1)S(1)}, bf16[8,2,32,512]{3,2,1,0:T(8,128)(2,1)S(1)}, u32[]{:S(2)}, u32[]{:S(2)}) collective-permute-start(bf16[8,2,32,512]{3,2,1,0:T(8,128)(2,1)S(1)} %all-to-all-done.1.own), channel_id=1, source_target_pairs={{448,0},{456,8},{464,16},{472,24},{480,32},{488,40},{496,48},{504,... | collective-permute-start | bytes 1572872 | tf_op jit(solution)/shard_map/ppermute | solution.py:80
  74.9 2.5 %collective-permute-start.1 = (bf16[8,2,32,512]{3,2,1,0:T(8,128)(2,1)S(1)}, bf16[8,2,32,512]{3,2,1,0:T(8,128)(2,1)S(1)}, u32[]{:S(2)}, u32[]{:S(2)}) collective-permute-start(bf16[8,2,32,512]{3,2,1,0:T(8,128)(2,1)S(1)} %all-to-all-done.1.own), channel_id=1, source_target_pairs={{8,0},{16,8},{24,16},{32,24},{40,32},{48,40},{56,48},{0,56},{72,64... | collective-permute-start | bytes 1572872 | tf_op jit(solution)/shard_map/ppermute | solution.py:80
  77.4 3.5 %all-to-all-done.2 = f16[64,4,512]{2,1,0:T(4,128)(2,1)S(1)} async-done(((f16[64,4,512]{2,1,0:T(4,128)(2,1)}), f16[64,4,512]{2,1,0:T(4,128)(2,1)S(1)}, u32[]{:S(2)}, u32[]{:S(2)}) %all-to-all-start.2) | async-done | bytes 262176 | tf_op jit(solution)/shard_map/all_to_all | solution.py:280
  81.1 0.8 broadcast_in_dim.8
  81.9 9.5 %all-to-all-start.3 = ((bf16[64,4,512]{2,1,0:T(4,128)(2,1)}), bf16[64,4,512]{2,1,0:T(4,128)(2,1)S(1)}, u32[]{:S(2)}, u32[]{:S(2)}) async-start(bf16[64,4,512]{2,1,0:T(4,128)(2,1)} %broadcast_in_dim.8), calls=%async_computation.3 | async-start | bytes 524288 | tf_op jit(solution)/shard_map/all_to_all | solution.py:60
  91.4 0.6 pad_add_fusion.place
  92.0 0.6 fusion.16
  92.6 0.6 fusion.17
  93.2 0.8 copy-done.5
  94.2 0.8 copy-done.7
  95.0 5.8 %arrange.1.weights = f32[2048,512]{1,0:T(8,128)} custom-call(s32[4]{0:T(128)} %pad_add_fusion.place, bf16[8,2,32,512]{3,2,1,0:T(8,128)(2,1)} %copy-done.1, bf16[8,2,32,512]{3,2,1,0:T(8,128)(2,1)} %copy-done.7, bf16[8,2,32,512]{3,2,1,0:T(8,128)(2,1)} %copy-done.6, bf16[8,2,32,512]{3,2,1,0:T(8,128)(2,1)} %copy-done.5), custom_call_target="tpu_custom_call" | custom-call | flops 62914560 | bytes 6291456 | tf_op jit(solution)/shard_map/arrange/pallas_call | solution.py:135
  100.8 4.1 %all-to-all-done.3.directions = bf16[64,4,512]{2,1,0:T(4,128)(2,1)S(1)} async-done(((bf16[64,4,512]{2,1,0:T(4,128)(2,1)}), bf16[64,4,512]{2,1,0:T(4,128)(2,1)S(1)}, u32[]{:S(2)}, u32[]{:S(2)}) %all-to-all-start.3) | async-done | bytes 262176 | tf_op jit(solution)/shard_map/all_to_all | solution.py:60
  104.9 0.7 copy-done.2
  105.6 6.1 %last_step.1 = (bf16[2048,256]{1,0:T(8,128)(2,1)}, bf16[256,2048]{1,0:T(8,128)(2,1)}, f32[32,256]{1,0:T(8,128)}, f32[32,256]{1,0:T(8,128)}) custom-call(f32[2048,512]{1,0:T(8,128)} %arrange.1.weights, bf16[64,4,512]{2,1,0:T(4,128)(2,1)} %copy-done.2, bf16[2048,256]{1,0:T(8,128)(2,1)} %value_factor.3, bf16[2048,256]{1,0:T(8,128)(2,1)} %output_factor.3, ...), custom_call_target="tpu_custom_call" | custom-call | tf_op jit(solution)/shard_map/last_step/pallas_call | solution.py:200
  (47 shorter events, 1.7 us)
Async XLA Ops:
  0.6 51.4 %copy-start = (bf16[512,256]{1,0:T(8,128)(2,1)S(1)}, bf16[512,256]{1,0:T(8,128)(2,1)}, u32[]{:S(2)}) copy-start(bf16[512,256]{1,0:T(8,128)(2,1)} %param.16) | copy-start | bytes 786436
  0.6 19.1 %copy-start.9 = (f32[32,256]{1,0:T(8,128)S(1)}, f32[32,256]{1,0:T(8,128)}, u32[]{:S(2)}) copy-start(f32[32,256]{1,0:T(8,128)} %value_weight.1) | copy-start | bytes 98308
  0.7 19.1 %copy-start.8 = (f32[256,32]{0,1:T(8,128)S(1)}, f32[256,32]{0,1:T(8,128)}, u32[]{:S(2)}) copy-start(f32[256,32]{0,1:T(8,128)} %param.25) | copy-start | bytes 98308
  0.7 18.5 %copy-start.14 = (f32[2]{0:T(128)S(1)}, f32[2]{0:T(128)}, u32[]{:S(2)}) copy-start(f32[2]{0:T(128)} %param.19) | copy-start | bytes 28
  0.7 19.1 %copy-start.3 = (bf16[512,256]{1,0:T(8,128)(2,1)S(1)}, bf16[512,256]{1,0:T(8,128)(2,1)}, u32[]{:S(2)}) copy-start(bf16[512,256]{1,0:T(8,128)(2,1)} %param.18) | copy-start | bytes 786436
  0.7 19.1 %copy-start.4 = (bf16[512,256]{1,0:T(8,128)(2,1)S(1)}, bf16[512,256]{1,0:T(8,128)(2,1)}, u32[]{:S(2)}) copy-start(bf16[512,256]{1,0:T(8,128)(2,1)} %param.17) | copy-start | bytes 786436
  0.7 20.6 %copy-start.15 = (f32[128]{0:T(128)S(1)}, f32[128]{0:T(128)}, u32[]{:S(2)}) copy-start(f32[128]{0:T(128)} %param.20) | copy-start | bytes 1540
  1.6 28.0 %collective-permute-start = (bf16[32,512]{1,0:T(8,128)(2,1)S(1)}, bf16[32,512]{1,0:T(8,128)(2,1)S(1)}, u32[]{:S(2)}, u32[]{:S(2)}) collective-permute-start(bf16[32,512]{1,0:T(8,128)(2,1)S(1)} %fusion.7), channel_id=1, source_target_pairs={{256,0},{264,8},{272,16},{280,24},{288,32},{296,40},{304,48},{312,... | collective-permute-start | bytes 98312 | tf_op jit(solution)/shard_map/ppermute | solution.py:80
  14.8 14.6 %all-to-all-start = ((bf16[8,64,512]{2,1,0:T(8,128)(2,1)}), bf16[8,64,512]{2,1,0:T(8,128)(2,1)S(1)}, u32[]{:S(2)}, u32[]{:S(2)}) async-start(bf16[8,64,512]{2,1,0:T(8,128)(2,1)} %project.1), calls=%async_computation | async-start | bytes 1048576 | tf_op jit(solution)/shard_map/all_to_all | solution.py:265
  30.4 25.7 %all-to-all-start.1 = ((bf16[8,2,32,512]{3,2,1,0:T(8,128)(2,1)}), bf16[8,2,32,512]{3,2,1,0:T(8,128)(2,1)S(1)}, u32[]{:S(2)}, u32[]{:S(2)}) async-start(bf16[8,2,32,512]{3,2,1,0:T(8,128)(2,1)} %broadcast_in_dim.7), calls=%async_computation.1 | async-start | bytes 1048576 | tf_op jit(solution)/shard_map/all_to_all | solution.py:60
  51.5 29.5 %copy-start.10 = (f32[4,256]{1,0:T(4,128)S(1)}, f32[4,256]{1,0:T(4,128)}, u32[]{:S(2)}) copy-start(f32[4,256]{1,0:T(4,128)} %param.29) | copy-start | bytes 12292
  51.5 29.5 %copy-start.11 = (f32[4,256]{1,0:T(4,128)S(1)}, f32[4,256]{1,0:T(4,128)}, u32[]{:S(2)}) copy-start(f32[4,256]{1,0:T(4,128)} %param.27) | copy-start | bytes 12292
  51.5 29.5 %copy-start.12 = (f32[4,256]{1,0:T(4,128)S(1)}, f32[4,256]{1,0:T(4,128)}, u32[]{:S(2)}) copy-start(f32[4,256]{1,0:T(4,128)} %param.28) | copy-start | bytes 12292
  51.5 29.5 %copy-start.13 = (f32[4,256]{1,0:T(4,128)S(1)}, f32[4,256]{1,0:T(4,128)}, u32[]{:S(2)}) copy-start(f32[4,256]{1,0:T(4,128)} %param.26) | copy-start | bytes 12292
  56.1 37.1 %copy-start.1 = (bf16[8,2,32,512]{3,2,1,0:T(8,128)(2,1)}, bf16[8,2,32,512]{3,2,1,0:T(8,128)(2,1)S(1)}, u32[]{:S(2)}) copy-start(bf16[8,2,32,512]{3,2,1,0:T(8,128)(2,1)S(1)} %all-to-all-done.1.own) | copy-start | bytes 1572868
  57.2 23.7 %all-to-all-start.2 = ((f16[64,4,512]{2,1,0:T(4,128)(2,1)}), f16[64,4,512]{2,1,0:T(4,128)(2,1)S(1)}, u32[]{:S(2)}, u32[]{:S(2)}) async-start(f16[64,4,512]{2,1,0:T(4,128)(2,1)} %reshape.176), calls=%async_computation.2 | async-start | bytes 524288 | tf_op jit(solution)/shard_map/all_to_all | solution.py:280
  67.2 26.0 %collective-permute-start.3 = (bf16[8,2,32,512]{3,2,1,0:T(8,128)(2,1)S(1)}, bf16[8,2,32,512]{3,2,1,0:T(8,128)(2,1)S(1)}, u32[]{:S(2)}, u32[]{:S(2)}) collective-permute-start(bf16[8,2,32,512]{3,2,1,0:T(8,128)(2,1)S(1)} %all-to-all-done.1.own), channel_id=1, source_target_pairs={{120,0},{64,8},{72,16},{80,24},{88,32},{96,40},{104,48},{112,56},{... | collective-permute-start | bytes 1572872 | tf_op jit(solution)/shard_map/ppermute | solution.py:80
  73.0 20.2 %collective-permute-start.2 = (bf16[8,2,32,512]{3,2,1,0:T(8,128)(2,1)S(1)}, bf16[8,2,32,512]{3,2,1,0:T(8,128)(2,1)S(1)}, u32[]{:S(2)}, u32[]{:S(2)}) collective-permute-start(bf16[8,2,32,512]{3,2,1,0:T(8,128)(2,1)S(1)} %all-to-all-done.1.own), channel_id=1, source_target_pairs={{448,0},{456,8},{464,16},{472,24},{480,32},{488,40},{496,48},{504,... | collective-permute-start | bytes 1572872 | tf_op jit(solution)/shard_map/ppermute | solution.py:80
  74.9 18.3 %collective-permute-start.1 = (bf16[8,2,32,512]{3,2,1,0:T(8,128)(2,1)S(1)}, bf16[8,2,32,512]{3,2,1,0:T(8,128)(2,1)S(1)}, u32[]{:S(2)}, u32[]{:S(2)}) collective-permute-start(bf16[8,2,32,512]{3,2,1,0:T(8,128)(2,1)S(1)} %all-to-all-done.1.own), channel_id=1, source_target_pairs={{8,0},{16,8},{24,16},{32,24},{40,32},{48,40},{56,48},{0,56},{72,64... | collective-permute-start | bytes 1572872 | tf_op jit(solution)/shard_map/ppermute | solution.py:80
  81.9 22.9 %all-to-all-start.3 = ((bf16[64,4,512]{2,1,0:T(4,128)(2,1)}), bf16[64,4,512]{2,1,0:T(4,128)(2,1)S(1)}, u32[]{:S(2)}, u32[]{:S(2)}) async-start(bf16[64,4,512]{2,1,0:T(4,128)(2,1)} %broadcast_in_dim.8), calls=%async_computation.3 | async-start | bytes 524288 | tf_op jit(solution)/shard_map/all_to_all | solution.py:60
  93.2 0.8 copy-start.5
  93.2 1.0 copy-start.6
  94.2 0.8 copy-start.7
  104.8 0.7 copy-start.2

commit v5 on v4

--- a/solution.py
+++ b/solution.py
@@ -48,11 +48,6 @@
 def two_parts(x):
     high = lax.reduce_precision(x, 8, 7)
     return high.astype(BF16), (x - high).astype(BF16)
-
-
-def dot_two(left, right_parts, left_dim, right_dim):
-    high, low = right_parts
-    return dot(left, high, left_dim, right_dim) + dot(left, low, left_dim, right_dim)
 
 
 def copy_for_each(x, axis):
@@ -146,6 +141,14 @@
     )(place, *quarters)
 
 
+def kept(x):
+    return pltpu.with_memory_space_constraint(x, pltpu.VMEM)
+
+
+def streamed(x):
+    return pltpu.with_memory_space_constraint(x, pltpu.HBM)
+
+
 def last_kernel(
     weights,
     directions,
@@ -159,68 +162,68 @@
     output_copy,
     value_master,
     output_master_t,
-    high,
-    low,
-    high_t,
-    low_t,
+    old,
+    value_factors,
+    output_factors,
+    value_rows,
+    output_columns,
+    in_sems,
+    sems,
 ):
-    cols = value_copy.shape[1]
-
-    @pl.when(pl.program_id(0) == 0)
-    def _():
-        whole = decoded(directions[...], 0.05 * DIRECTION_LIMIT).reshape(high.shape[0], -1)
-        value = whole[:, :cols]
-        upper = value.astype(BF16)
-        high[...] = upper
-        low[...] = (value - upper.astype(F32)).astype(BF16)
-        output = whole[:, cols:].T
-        upper = output.astype(BF16)
-        high_t[...] = upper
-        low_t[...] = (output - upper.astype(F32)).astype(BF16)
-        value_master[...] = value_weight[...] - (
-            dot(own_value_factor[...], high[...], 1, 0) + dot(own_value_factor[...], low[...], 1, 0)
-        )
-        output_master_t[...] = output_weight_t[...] - (
-            dot(own_output_factor[...], high_t[...], 1, 1)
-            + dot(own_output_factor[...], low_t[...], 1, 1)
-        )
-
-    value_step = dot(value_factor[...], high[...], 1, 0) + dot(value_factor[...], low[...], 1, 0)
-    value_copy[...] = (weights[:, :cols] - value_step).astype(BF16)
-    output_step = dot(high_t[...], output_factor[...], 1, 1) + dot(
-        low_t[...], output_factor[...], 1, 1
-    )
-    output_copy[...] = (weights[:, cols:].T - output_step).astype(BF16)
+    width, cols = value_rows.shape
+    rank = value_factor.shape[1]
+    loads = []
+    for step in range(width // GROUP):
+        rows = pl.ds(step * GROUP, GROUP)
+        arrays = ((value_factor, value_factors), (weights, old), (output_factor, output_factors))
+        for i, (array, held) in enumerate(arrays):
+            loads.append(pltpu.make_async_copy(array.at[rows, :], held.at[rows, :], in_sems.at[i, step]))
+            loads[-1].start()
+    whole = decoded(directions[...], 0.05 * DIRECTION_LIMIT).reshape(rank, 2 * cols)
+    high = whole[:, :cols].astype(BF16)
+    low = (whole[:, :cols] - high.astype(F32)).astype(BF16)
+    turned = whole[:, cols:].T
+    high_t = turned.astype(BF16)
+    low_t = (turned - high_t.astype(F32)).astype(BF16)
+    copies = []
+    for step in range(width // GROUP):
+        rows = slice(step * GROUP, (step + 1) * GROUP)
+        for load in loads[3 * step : 3 * step + 3]:
+            load.wait()
+        factor = value_factors[rows, :]
+        value_step = dot(factor, high, 1, 0) + dot(factor, low, 1, 0)
+        value_rows[rows, :] = (old[rows, :cols] - value_step).astype(BF16)
+        copies.append(pltpu.make_async_copy(value_rows.at[rows, :], value_copy.at[rows, :], sems.at[0, step]))
+        copies[-1].start()
+        factor = output_factors[rows, :]
+        output_step = dot(high_t, factor, 1, 1) + dot(low_t, factor, 1, 1)
+        output_columns[:, rows] = (old[rows, cols:].T - output_step).astype(BF16)
+        copies.append(pltpu.make_async_copy(output_columns.at[:, rows], output_copy.at[:, rows], sems.at[1, step]))
+        copies[-1].start()
+    factor = own_value_factor[...]
+    value_master[...] = value_weight[...] - (dot(factor, high, 1, 0) + dot(factor, low, 1, 0))
+    factor = own_output_factor[...]
+    output_master_t[...] = output_weight_t[...] - (dot(factor, high_t, 1, 1) + dot(factor, low_t, 1, 1))
+    for copy in copies:
+        copy.wait()
 
 
 def last_step(weights, directions, value_factor, output_factor, own_v, own_o, value_weight, output_weight_t):
-    width, rank = value_factor.shape
+    width = value_factor.shape[0]
     rows, cols = value_weight.shape
-    whole = lambda *shape: pl.BlockSpec(shape, lambda i: (0,) * len(shape))
+    in_vmem, in_hbm = pl.BlockSpec(memory_space=pltpu.VMEM), pl.BlockSpec(memory_space=pltpu.HBM)
     return pl.pallas_call(
         last_kernel,
-        grid=(width // GROUP,),
-        in_specs=[
-            pl.BlockSpec((GROUP, 2 * cols), lambda i: (i, 0)),
-            whole(*directions.shape),
-            pl.BlockSpec((GROUP, rank), lambda i: (i, 0)),
-            pl.BlockSpec((GROUP, rank), lambda i: (i, 0)),
-            whole(*own_v.shape),
-            whole(*own_o.shape),
-            whole(rows, cols),
-            whole(rows, cols),
-        ],
-        out_specs=[
-            pl.BlockSpec((GROUP, cols), lambda i: (i, 0)),
-            pl.BlockSpec((cols, GROUP), lambda i: (0, i)),
-            whole(rows, cols),
-            whole(rows, cols),
-        ],
+        in_specs=[in_hbm, in_vmem, in_hbm, in_hbm] + [in_vmem] * 4,
+        out_specs=[in_hbm, in_hbm, in_vmem, in_vmem],
         scratch_shapes=[
-            pltpu.VMEM((rank, cols), BF16),
-            pltpu.VMEM((rank, cols), BF16),
-            pltpu.VMEM((cols, rank), BF16),
-            pltpu.VMEM((cols, rank), BF16),
+            pltpu.VMEM(weights.shape, F32),
+            pltpu.VMEM(value_factor.shape, BF16),
+            pltpu.VMEM(output_factor.shape, BF16),
+            pltpu.VMEM((width, cols), BF16),
+            pltpu.VMEM((cols, width), BF16),
+            pltpu.SemaphoreType.DMA((3, width // GROUP)),
+            pltpu.SemaphoreType.DMA((2, width // GROUP)),
         ],
         out_shape=[
             jax.ShapeDtypeStruct((width, cols), BF16),
@@ -229,7 +232,16 @@
             jax.ShapeDtypeStruct((rows, cols), F32),
         ],
         name="last_step",
-    )(weights, directions, value_factor, output_factor, own_v, own_o, value_weight, output_weight_t)
+    )(
+        streamed(weights),
+        kept(directions),
+        streamed(value_factor),
+        streamed(output_factor),
+        own_v,
+        own_o,
+        value_weight,
+        output_weight_t,
+    )
 
 
 def update(
@@ -271,9 +283,12 @@
     heads_out = normed_heads(first_map, second_map, lambdas, head_gain)
     scale = LOW_SCALE / (TOKEN_SCALE * math.sqrt(tok_rows * fs_size))
     token_parts = two_parts(tokens)
-    low_value = dot_two(value_cotangent, [p[:, :rank] for p in token_parts], 0, 0)
-    low_output = dot_two(heads_out, [p[:, rank:] for p in token_parts], 0, 0)
-    partial = jnp.concatenate([low_value.T, low_output.T], axis=1) * scale
+    low = []
+    for side, right in enumerate((value_cotangent, heads_out)):
+        columns = slice(side * rank, (side + 1) * rank)
+        both = dot(jnp.concatenate([p[:, columns] for p in token_parts], axis=1), right, 0, 0)
+        low.append(both[:rank] + both[rank:])
+    partial = jnp.concatenate(low, axis=1) * scale
     partial, own_quarter = lax.optimization_barrier((partial, own_quarter))
     weights = all_quarters(own_quarter)
     tiles = partial.astype(F16).reshape(fs_size, -1, 2 * cols)

time: 112 us -> 111 us (level)
    unnamed x32 -> x30, local copies, waits for them, and re-layouts: 2.54 us -> 1.84 us
where the time goes in v5:
time: 111 us
  starting transfers between devices  51.2 us (46%)
  waiting for transfers between devices  17.7 us (16%)
  Pallas kernels  14 us (13%)
  blocking collectives  13.1 us (12%)
  local copies, waits for them, and re-layouts  7.74 us (7%)
  other arithmetic  5.11 us (5%)
    ppermute x4, starting transfers between devices, from_offset(): return lax.ppermute(x, FS, pairs)  21.1 us
    all_to_all x2, starting transfers between devices, copy_for_each(): lax.all_to_all(jnp.broadcast_to(x[None], (size, *x.shape)), axis, 0, 0, t...  17.5 us
    all_gather x1, blocking collectives, update(): tokens = lax.all_gather(summed, 'tp', axis=0, tiled=True).astype(F32)  13.1 us
    all_to_all x1, starting transfers between devices, update(): tiles = lax.all_to_all(tiles, FS, 0, 0, tiled=True)  8.39 us
    all_to_all x2, waiting for transfers between devices, copy_for_each(): lax.all_to_all(jnp.broadcast_to(x[None], (size, *x.shape)), axis, 0, 0, t...  7.55 us
    all_to_all x1, waiting for transfers between devices, update(): pieces = lax.all_to_all(pieces, 'tp', 0, 0, tiled=True)  6.61 us
    pallas_call x1, Pallas kernels, last_step(): pl.pallas_call(last_kernel, in_specs=[in_hbm, in_vmem, in_hbm, in_hbm] +...  5.96 us
    pallas_call x1, Pallas kernels, arrange(): pl.pallas_call(arrange_kernel, grid_spec=pltpu.PrefetchScalarGridSpec(num...  5.76 us
  transfers between devices with their start and end apart: 8, of which 4 were waited for; matrix products, arithmetic and copies ran while one was open for 8% of the time, Pallas kernels for 7%

profile of v5, /device:TPU:8, one launch (start us, length us, event | category | flops | bytes accessed | tf_op | source)
XLA Modules:
  0.0 110.6 jit_solution(13664909783523324913)
XLA Ops:
  0.7 0.9 fusion.12
  1.6 10.9 %collective-permute-start = (bf16[32,512]{1,0:T(8,128)(2,1)S(1)}, bf16[32,512]{1,0:T(8,128)(2,1)S(1)}, u32[]{:S(2)}, u32[]{:S(2)}) collective-permute-start(bf16[32,512]{1,0:T(8,128)(2,1)S(1)} %fusion.12), channel_id=1, source_target_pairs={{256,0},{264,8},{272,16},{280,24},{288,32},{296,40},{304,48},{312,... | collective-permute-start | bytes 98312 | tf_op jit(solution)/shard_map/ppermute | solution.py:75
  12.5 2.3 %project.1 = bf16[8,64,512]{2,1,0:T(8,128)(2,1)} custom-call(s32[1]{0:T(128)} %bitcast.2.place, bf16[512,256]{1,0:T(8,128)(2,1)} %inputs.1, bf16[512,256]{1,0:T(8,128)(2,1)} %cotangent.1, bf16[2048,256]{1,0:T(8,128)(2,1)} %value_factor.3, bf16[2048,256]{1,0:T(8,128)(2,1)} %output_factor.3), custom_call_target="tpu_custom_call" | custom-call | tf_op jit(solution)/shard_map/project/pallas_call | solution.py:92
  14.8 4.3 %all-to-all-start = ((bf16[8,64,512]{2,1,0:T(8,128)(2,1)}), bf16[8,64,512]{2,1,0:T(8,128)(2,1)S(1)}, u32[]{:S(2)}, u32[]{:S(2)}) async-start(bf16[8,64,512]{2,1,0:T(8,128)(2,1)} %project.1), calls=%async_computation | async-start | bytes 1048576 | tf_op jit(solution)/shard_map/all_to_all | solution.py:277
  19.1 0.6 fusion.25
  19.8 1.5 %multiply_reduce_fusion.1 = (f32[512]{0:T(512)S(1)}, f32[512]{0:T(512)S(1)}) fusion(f32[]{:T(128)} %bitcast.4, bf16[512,256]{1,0:T(8,128)(2,1)S(1)} %copy-done.2, bf16[512,256]{1,0:T(8,128)(2,1)S(1)} %copy-done.3, f32[]{:T(128)} %bitcast.5), kind=kLoop, calls=%fused_computation.23 | loop fusion | flops 785408 | bytes 528392 | tf_op jit(solution)/shard_map/reduce_sum | solution.py:64
  21.3 1.5 %multiply_convert_fusion.1 = (bf16[512,128]{1,0:T(8,128)(2,1)S(1)}, bf16[512,128]{1,0:T(8,128)(2,1)S(1)}) fusion(f32[128]{0:T(128)S(1)} %copy-done.14, f32[512]{0:T(512)S(1)} %get-tuple-element.46, f32[]{:T(128)} %bitcast.4, bf16[512,256]{1,0:T(8,128)(2,1)S(1)} %copy-done.2, bf16[512,256]{1,0:T(8,128)(2,1)S(1)} %copy-done.3, f32[512]{0:T(512)S(1)} %get-tuple-element.45, ...), kind=kLoop, calls=%fused_computation.22 | loop fusion | flops 917504 | bytes 791048 | tf_op jit(solution)/shard_map/convert_element_type | solution.py:65
  22.8 6.6 %all-to-all-done = bf16[8,64,512]{2,1,0:T(8,128)(2,1)S(1)} async-done(((bf16[8,64,512]{2,1,0:T(8,128)(2,1)}), bf16[8,64,512]{2,1,0:T(8,128)(2,1)S(1)}, u32[]{:S(2)}, u32[]{:S(2)}) %all-to-all-start) | async-done | bytes 524320 | tf_op jit(solution)/shard_map/all_to_all | solution.py:277
  29.6 0.8 broadcast_in_dim.7
  30.4 8.0 %all-to-all-start.1 = ((bf16[8,2,32,512]{3,2,1,0:T(8,128)(2,1)}), bf16[8,2,32,512]{3,2,1,0:T(8,128)(2,1)S(1)}, u32[]{:S(2)}, u32[]{:S(2)}) async-start(bf16[8,2,32,512]{3,2,1,0:T(8,128)(2,1)} %broadcast_in_dim.7), calls=%async_computation.1 | async-start | bytes 1048576 | tf_op jit(solution)/shard_map/all_to_all | solution.py:55
  38.4 13.1 %all_gather.3 = f16[512,512]{1,0:T(8,128)(2,1)S(1)} all-gather(f16[64,512]{1,0:T(8,128)(2,1)S(1)} %multiply_convert_fusion.2), channel_id=1, replica_groups=mesh['z_far'=2,'z_high'=2,'z_low'=2,'y_high'=4,'y_low'=2,'tp'=8] {'tp'}, dimensions={0}, use_global_device_ids=true | all-gather | bytes 589824 | tf_op jit(solution)/shard_map/all_gather | solution.py:281
  51.8 0.3 fusion.5
  52.2 0.3 fusion.1
  52.7 3.5 %all-to-all-done.1.own = bf16[8,2,32,512]{3,2,1,0:T(8,128)(2,1)S(1)} async-done(((bf16[8,2,32,512]{3,2,1,0:T(8,128)(2,1)}), bf16[8,2,32,512]{3,2,1,0:T(8,128)(2,1)S(1)}, u32[]{:S(2)}, u32[]{:S(2)}) %all-to-all-start.1) | async-done | bytes 524320 | tf_op jit(solution)/shard_map/all_to_all | solution.py:55
  56.2 0.3 copy.23
  56.5 0.8 reshape.176
  57.2 8.4 %all-to-all-start.2 = ((f16[64,4,512]{2,1,0:T(4,128)(2,1)}), f16[64,4,512]{2,1,0:T(4,128)(2,1)S(1)}, u32[]{:S(2)}, u32[]{:S(2)}) async-start(f16[64,4,512]{2,1,0:T(4,128)(2,1)} %reshape.176), calls=%async_computation.2 | async-start | bytes 524288 | tf_op jit(solution)/shard_map/all_to_all | solution.py:295
  65.7 1.4 %constant_dynamic-slice_fusion = (bf16[32,256]{1,0:T(8,128)(2,1)}, bf16[32,256]{1,0:T(8,128)(2,1)}) fusion(bf16[2048,256]{1,0:T(8,128)(2,1)} %output_factor.3, s32[]{:T(128)S(6)} %select_n.28, bf16[2048,256]{1,0:T(8,128)(2,1)} %value_factor.3), kind=kLoop, calls=%fused_computation.43 | loop fusion | bytes 65540 | tf_op jit(solution)/shard_map/dynamic_slice | solution.py:306
  67.0 5.7 %collective-permute-start.3 = (bf16[8,2,32,512]{3,2,1,0:T(8,128)(2,1)S(1)}, bf16[8,2,32,512]{3,2,1,0:T(8,128)(2,1)S(1)}, u32[]{:S(2)}, u32[]{:S(2)}) collective-permute-start(bf16[8,2,32,512]{3,2,1,0:T(8,128)(2,1)S(1)} %all-to-all-done.1.own), channel_id=1, source_target_pairs={{120,0},{64,8},{72,16},{80,24},{88,32},{96,40},{104,48},{112,56},{... | collective-permute-start | bytes 1572872 | tf_op jit(solution)/shard_map/ppermute | solution.py:75
  72.8 1.9 %collective-permute-start.2 = (bf16[8,2,32,512]{3,2,1,0:T(8,128)(2,1)S(1)}, bf16[8,2,32,512]{3,2,1,0:T(8,128)(2,1)S(1)}, u32[]{:S(2)}, u32[]{:S(2)}) collective-permute-start(bf16[8,2,32,512]{3,2,1,0:T(8,128)(2,1)S(1)} %all-to-all-done.1.own), channel_id=1, source_target_pairs={{448,0},{456,8},{464,16},{472,24},{480,32},{488,40},{496,48},{504,... | collective-permute-start | bytes 1572872 | tf_op jit(solution)/shard_map/ppermute | solution.py:75
  74.7 2.5 %collective-permute-start.1 = (bf16[8,2,32,512]{3,2,1,0:T(8,128)(2,1)S(1)}, bf16[8,2,32,512]{3,2,1,0:T(8,128)(2,1)S(1)}, u32[]{:S(2)}, u32[]{:S(2)}) collective-permute-start(bf16[8,2,32,512]{3,2,1,0:T(8,128)(2,1)S(1)} %all-to-all-done.1.own), channel_id=1, source_target_pairs={{8,0},{16,8},{24,16},{32,24},{40,32},{48,40},{56,48},{0,56},{72,64... | collective-permute-start | bytes 1572872 | tf_op jit(solution)/shard_map/ppermute | solution.py:75
  77.2 3.5 %all-to-all-done.2 = f16[64,4,512]{2,1,0:T(4,128)(2,1)S(1)} async-done(((f16[64,4,512]{2,1,0:T(4,128)(2,1)}), f16[64,4,512]{2,1,0:T(4,128)(2,1)S(1)}, u32[]{:S(2)}, u32[]{:S(2)}) %all-to-all-start.2) | async-done | bytes 262176 | tf_op jit(solution)/shard_map/all_to_all | solution.py:295
  80.9 0.8 broadcast_in_dim.8
  81.7 9.5 %all-to-all-start.3 = ((bf16[64,4,512]{2,1,0:T(4,128)(2,1)}), bf16[64,4,512]{2,1,0:T(4,128)(2,1)S(1)}, u32[]{:S(2)}, u32[]{:S(2)}) async-start(bf16[64,4,512]{2,1,0:T(4,128)(2,1)} %broadcast_in_dim.8), calls=%async_computation.3 | async-start | bytes 524288 | tf_op jit(solution)/shard_map/all_to_all | solution.py:55
  91.2 0.6 pad_add_fusion.place
  91.8 0.6 fusion.23
  92.4 0.6 fusion.24
  93.0 0.8 copy-done.4
  94.0 0.8 copy-done.6
  94.8 5.8 %arrange.1.weights = f32[2048,512]{1,0:T(8,128)} custom-call(s32[4]{0:T(128)} %pad_add_fusion.place, bf16[8,2,32,512]{3,2,1,0:T(8,128)(2,1)} %copy-done.1, bf16[8,2,32,512]{3,2,1,0:T(8,128)(2,1)} %copy-done.6, bf16[8,2,32,512]{3,2,1,0:T(8,128)(2,1)} %copy-done.5, bf16[8,2,32,512]{3,2,1,0:T(8,128)(2,1)} %copy-done.4), custom_call_target="tpu_custom_call" | custom-call | flops 62914560 | bytes 6291456 | tf_op jit(solution)/shard_map/arrange/pallas_call | solution.py:130
  100.5 4.1 %all-to-all-done.3.directions = bf16[64,4,512]{2,1,0:T(4,128)(2,1)S(1)} async-done(((bf16[64,4,512]{2,1,0:T(4,128)(2,1)}), bf16[64,4,512]{2,1,0:T(4,128)(2,1)S(1)}, u32[]{:S(2)}, u32[]{:S(2)}) %all-to-all-start.3) | async-done | bytes 262176 | tf_op jit(solution)/shard_map/all_to_all | solution.py:55
  104.6 6.0 %last_step.1 = (bf16[2048,256]{1,0:T(8,128)(2,1)}, bf16[256,2048]{1,0:T(8,128)(2,1)}, f32[32,256]{1,0:T(8,128)}, f32[32,256]{1,0:T(8,128)}) custom-call(f32[2048,512]{1,0:T(8,128)} %arrange.1.weights, bf16[64,4,512]{2,1,0:T(4,128)(2,1)S(1)} %all-to-all-done.3.directions, bf16[2048,256]{1,0:T(8,128)(2,1)} %value_factor.3, bf16[2048,256]{1,0:T(8,128)(2,1)} %output_factor.3, ...), custom_call_target="tpu_custom_call" | custom-call | tf_op jit(solution)/shard_map/last_step/pallas_call | solution.py:215
  (46 shorter events, 1.0 us)
Async XLA Ops:
  0.6 51.5 %copy-start = (bf16[512,256]{1,0:T(8,128)(2,1)S(1)}, bf16[512,256]{1,0:T(8,128)(2,1)}, u32[]{:S(2)}) copy-start(bf16[512,256]{1,0:T(8,128)(2,1)} %param.16) | copy-start | bytes 786436
  0.6 19.1 %copy-start.8 = (f32[32,256]{1,0:T(8,128)S(1)}, f32[32,256]{1,0:T(8,128)}, u32[]{:S(2)}) copy-start(f32[32,256]{1,0:T(8,128)} %value_weight.1) | copy-start | bytes 98308
  0.7 19.1 %copy-start.7 = (f32[256,32]{0,1:T(8,128)S(1)}, f32[256,32]{0,1:T(8,128)}, u32[]{:S(2)}) copy-start(f32[256,32]{0,1:T(8,128)} %param.25) | copy-start | bytes 98308
  0.7 18.5 %copy-start.13 = (f32[2]{0:T(128)S(1)}, f32[2]{0:T(128)}, u32[]{:S(2)}) copy-start(f32[2]{0:T(128)} %param.19) | copy-start | bytes 28
  0.7 19.1 %copy-start.2 = (bf16[512,256]{1,0:T(8,128)(2,1)S(1)}, bf16[512,256]{1,0:T(8,128)(2,1)}, u32[]{:S(2)}) copy-start(bf16[512,256]{1,0:T(8,128)(2,1)} %param.18) | copy-start | bytes 786436
  0.7 19.1 %copy-start.3 = (bf16[512,256]{1,0:T(8,128)(2,1)S(1)}, bf16[512,256]{1,0:T(8,128)(2,1)}, u32[]{:S(2)}) copy-start(bf16[512,256]{1,0:T(8,128)(2,1)} %param.17) | copy-start | bytes 786436
  0.7 20.6 %copy-start.14 = (f32[128]{0:T(128)S(1)}, f32[128]{0:T(128)}, u32[]{:S(2)}) copy-start(f32[128]{0:T(128)} %param.20) | copy-start | bytes 1540
  1.6 28.0 %collective-permute-start = (bf16[32,512]{1,0:T(8,128)(2,1)S(1)}, bf16[32,512]{1,0:T(8,128)(2,1)S(1)}, u32[]{:S(2)}, u32[]{:S(2)}) collective-permute-start(bf16[32,512]{1,0:T(8,128)(2,1)S(1)} %fusion.12), channel_id=1, source_target_pairs={{256,0},{264,8},{272,16},{280,24},{288,32},{296,40},{304,48},{312,... | collective-permute-start | bytes 98312 | tf_op jit(solution)/shard_map/ppermute | solution.py:75
  14.8 14.6 %all-to-all-start = ((bf16[8,64,512]{2,1,0:T(8,128)(2,1)}), bf16[8,64,512]{2,1,0:T(8,128)(2,1)S(1)}, u32[]{:S(2)}, u32[]{:S(2)}) async-start(bf16[8,64,512]{2,1,0:T(8,128)(2,1)} %project.1), calls=%async_computation | async-start | bytes 1048576 | tf_op jit(solution)/shard_map/all_to_all | solution.py:277
  30.4 25.7 %all-to-all-start.1 = ((bf16[8,2,32,512]{3,2,1,0:T(8,128)(2,1)}), bf16[8,2,32,512]{3,2,1,0:T(8,128)(2,1)S(1)}, u32[]{:S(2)}, u32[]{:S(2)}) async-start(bf16[8,2,32,512]{3,2,1,0:T(8,128)(2,1)} %broadcast_in_dim.7), calls=%async_computation.1 | async-start | bytes 1048576 | tf_op jit(solution)/shard_map/all_to_all | solution.py:55
  51.8 29.1 %copy-start.9 = (f32[4,256]{1,0:T(4,128)S(1)}, f32[4,256]{1,0:T(4,128)}, u32[]{:S(2)}) copy-start(f32[4,256]{1,0:T(4,128)} %param.29) | copy-start | bytes 12292
  51.8 29.1 %copy-start.10 = (f32[4,256]{1,0:T(4,128)S(1)}, f32[4,256]{1,0:T(4,128)}, u32[]{:S(2)}) copy-start(f32[4,256]{1,0:T(4,128)} %param.27) | copy-start | bytes 12292
  51.8 29.1 %copy-start.11 = (f32[4,256]{1,0:T(4,128)S(1)}, f32[4,256]{1,0:T(4,128)}, u32[]{:S(2)}) copy-start(f32[4,256]{1,0:T(4,128)} %param.28) | copy-start | bytes 12292
  51.8 29.0 %copy-start.12 = (f32[4,256]{1,0:T(4,128)S(1)}, f32[4,256]{1,0:T(4,128)}, u32[]{:S(2)}) copy-start(f32[4,256]{1,0:T(4,128)} %param.26) | copy-start | bytes 12292
  56.1 36.9 %copy-start.1 = (bf16[8,2,32,512]{3,2,1,0:T(8,128)(2,1)}, bf16[8,2,32,512]{3,2,1,0:T(8,128)(2,1)S(1)}, u32[]{:S(2)}) copy-start(bf16[8,2,32,512]{3,2,1,0:T(8,128)(2,1)S(1)} %all-to-all-done.1.own) | copy-start | bytes 1572868
  57.2 23.4 %all-to-all-start.2 = ((f16[64,4,512]{2,1,0:T(4,128)(2,1)}), f16[64,4,512]{2,1,0:T(4,128)(2,1)S(1)}, u32[]{:S(2)}, u32[]{:S(2)}) async-start(f16[64,4,512]{2,1,0:T(4,128)(2,1)} %reshape.176), calls=%async_computation.2 | async-start | bytes 524288 | tf_op jit(solution)/shard_map/all_to_all | solution.py:295
  67.0 26.0 %collective-permute-start.3 = (bf16[8,2,32,512]{3,2,1,0:T(8,128)(2,1)S(1)}, bf16[8,2,32,512]{3,2,1,0:T(8,128)(2,1)S(1)}, u32[]{:S(2)}, u32[]{:S(2)}) collective-permute-start(bf16[8,2,32,512]{3,2,1,0:T(8,128)(2,1)S(1)} %all-to-all-done.1.own), channel_id=1, source_target_pairs={{120,0},{64,8},{72,16},{80,24},{88,32},{96,40},{104,48},{112,56},{... | collective-permute-start | bytes 1572872 | tf_op jit(solution)/shard_map/ppermute | solution.py:75
  72.8 20.2 %collective-permute-start.2 = (bf16[8,2,32,512]{3,2,1,0:T(8,128)(2,1)S(1)}, bf16[8,2,32,512]{3,2,1,0:T(8,128)(2,1)S(1)}, u32[]{:S(2)}, u32[]{:S(2)}) collective-permute-start(bf16[8,2,32,512]{3,2,1,0:T(8,128)(2,1)S(1)} %all-to-all-done.1.own), channel_id=1, source_target_pairs={{448,0},{456,8},{464,16},{472,24},{480,32},{488,40},{496,48},{504,... | collective-permute-start | bytes 1572872 | tf_op jit(solution)/shard_map/ppermute | solution.py:75
  74.7 18.3 %collective-permute-start.1 = (bf16[8,2,32,512]{3,2,1,0:T(8,128)(2,1)S(1)}, bf16[8,2,32,512]{3,2,1,0:T(8,128)(2,1)S(1)}, u32[]{:S(2)}, u32[]{:S(2)}) collective-permute-start(bf16[8,2,32,512]{3,2,1,0:T(8,128)(2,1)S(1)} %all-to-all-done.1.own), channel_id=1, source_target_pairs={{8,0},{16,8},{24,16},{32,24},{40,32},{48,40},{56,48},{0,56},{72,64... | collective-permute-start | bytes 1572872 | tf_op jit(solution)/shard_map/ppermute | solution.py:75
  81.7 22.9 %all-to-all-start.3 = ((bf16[64,4,512]{2,1,0:T(4,128)(2,1)}), bf16[64,4,512]{2,1,0:T(4,128)(2,1)S(1)}, u32[]{:S(2)}, u32[]{:S(2)}) async-start(bf16[64,4,512]{2,1,0:T(4,128)(2,1)} %broadcast_in_dim.8), calls=%async_computation.3 | async-start | bytes 524288 | tf_op jit(solution)/shard_map/all_to_all | solution.py:55
  93.0 0.8 copy-start.4
  93.0 1.0 copy-start.5
  94.0 0.8 copy-start.6
